TPU v7x, 128 devices: a whole 4x4x4 slice. The times are simulated.
128 devices in a mesh: dp: 4 (over x), kv: 16 (over z, y), tp: 2 (over core).
Axes of the slice: x: 4, y: 4, z: 4, core: 2. Of those that a mesh axis runs over, the one named last changes fastest.
Arguments:
- tokens: bfloat16 [1024, 4096], P('dp', ('kv', 'tp')), may hold values from -53 to 53
- carried_state: float32 [1024, 16, 128, 128], P(('dp', 'kv', 'tp')), may hold values from -9 to 9
- first_gain: float32 [4096], replicated, may hold values from 0.1 to 1.9
- first_gate: bfloat16 [4096, 11264], P(None, ('kv', 'tp')), may hold values from -0.09375 to 0.09375
- first_up: bfloat16 [4096, 11264], P(None, ('kv', 'tp')), may hold values from -0.09375 to 0.09375
- first_down: bfloat16 [11264, 4096], P(('kv', 'tp')), may hold values from -0.109375 to 0.109375
- mix_gain: float32 [4096], replicated, may hold values from 0.1 to 1.9
- query_weight: bfloat16 [4096, 2048], P(('kv', 'tp')), may hold values from -0.09375 to 0.09375
- forget_weight: bfloat16 [4096, 2048], P(('kv', 'tp')), may hold values from -0.09375 to 0.09375
- input_weight: bfloat16 [4096, 2048], P(('kv', 'tp')), may hold values from -0.09375 to 0.09375
- outgate_weight: bfloat16 [4096, 2048], P(('kv', 'tp')), may hold values from -0.09375 to 0.09375
- forget_floor: float32 [2048], replicated, may hold values from 0.05 to 0.9
- head_gain: float32 [128], replicated, may hold values from 0.1 to 1.9
- output_weight: bfloat16 [2048, 4096], P(None, ('kv', 'tp')), may hold values from -0.125 to 0.125
- second_gain: float32 [4096], replicated, may hold values from 0.1 to 1.9
- second_gate: bfloat16 [4096, 11264], P(None, ('kv', 'tp')), may hold values from -0.09375 to 0.09375
- second_up: bfloat16 [4096, 11264], P(None, ('kv', 'tp')), may hold values from -0.09375 to 0.09375
- second_down: bfloat16 [11264, 4096], P(('kv', 'tp')), may hold values from -0.109375 to 0.109375
Outputs:
- layer_out: bfloat16 [1024, 4096], P('dp', ('kv', 'tp'))
- next_state: float32 [1024, 16, 128, 128], P(('dp', 'kv', 'tp'))
All inputs are finite; a program needn't handle non-finite values.
Results may differ from a plain program's by a relative error of at most 0.018.
Values may be sent and summed in bfloat16 or wider, within the bound.
A program may use at most 128 MiB of HBM per device.

v0:
```python
import jax
import jax.numpy as jnp
from jax import lax
from jax.sharding import Mesh
from jax.sharding import PartitionSpec as P

KV_TP = ("kv_0", "kv_1", "tp")
DP_KV_TP = ("dp", "kv_0", "kv_1", "tp")


epsilon = 1e-06


def copy_for_each(shard, axis):
    devices = lax.axis_size(axis)
    return lax.all_to_all(
        jnp.broadcast_to(shard[None], (devices, *shard.shape)), axis, 0, 0, tiled=True
    )


def joined_along(parts, dim):
    parts = jnp.moveaxis(parts, 0, dim)
    lengths = parts.shape
    return parts.reshape(*lengths[:dim], lengths[dim] * lengths[dim + 1], *lengths[dim + 2 :])


def whole_of(shard, axes, dim):
    far, near = axes
    parts = copy_for_each(copy_for_each(shard, far), near)
    return joined_along(parts.swapaxes(0, 1).reshape(-1, *shard.shape), dim)


def in_blocks(shard, dim, devices):
    before, after = (shard.shape[:dim], shard.shape[dim + 1 :])
    return jnp.moveaxis(shard.reshape(*before, devices, -1, *after), dim, 0)


def sum_at_owner(shard, axis, dim):
    devices = lax.axis_size(axis)
    parts = lax.all_to_all(in_blocks(shard, dim, devices), axis, 0, 0, tiled=True)
    return jnp.sum(parts, axis=0)


def sum_in_two_steps(shard, axes, dim):
    far, near = axes
    own = sum_at_owner(in_blocks(shard, dim, lax.axis_size(far)), near, dim + 1)
    return jnp.sum(lax.all_to_all(own, far, 0, 0, tiled=True), axis=0)


def of_everyone(shard, axis):
    return copy_for_each(shard, axis).sum(axis=0)


def sent_and_summed(shard, axis, dim):
    devices = lax.axis_size(axis)
    parts = lax.all_to_all(in_blocks(shard, dim, devices), axis, 0, 0, tiled=True)
    return jnp.sum(parts.astype(jnp.float32), axis=0)


def sum_by_axis(shard, axes, dim):
    far, near = axes
    parts = in_blocks(shard, dim, lax.axis_size(far))
    nearer = sent_and_summed(parts, near, dim + 1)
    arrived = lax.all_to_all(
        nearer.astype(jnp.bfloat16), far, split_axis=0, concat_axis=0, tiled=True
    )
    return arrived.astype(jnp.float32).sum(axis=0)


def collect(shard, axis, dim):
    return joined_along(copy_for_each(shard, axis), dim)


def fold_step(gain_vec, gate_weight, up_weight, block_cols):
    widened = block_cols.astype(jnp.float32)
    scaled = (widened * gain_vec).astype(jnp.bfloat16)
    gate_acc = jnp.dot(scaled, gate_weight, preferred_element_type=jnp.float32)
    up_acc = jnp.dot(scaled, up_weight, preferred_element_type=jnp.float32)
    squares = jnp.sum(widened * widened, axis=1)
    return (gate_acc, up_acc, squares)


def channel_terms(own_cols, totals, down_weight, own_index, full_width):
    gate_acc, up_acc, squares = totals
    row_scale = lax.rsqrt(squares / full_width + epsilon)[:, None]
    hidden = (jax.nn.silu(row_scale * gate_acc) * (row_scale * up_acc)).astype(jnp.bfloat16)
    branch_sum = 0.5 * jnp.dot(hidden, down_weight, preferred_element_type=jnp.float32)
    own_part = lax.dynamic_update_slice_in_dim(
        jnp.zeros_like(branch_sum), own_cols.astype(jnp.float32), own_index * own_cols.shape[1], 1
    )
    return branch_sum + own_part


def per_device(
    tokens,
    carried_state,
    first_gain,
    first_gate,
    first_up,
    first_down,
    mix_gain,
    query_weight,
    forget_weight,
    input_weight,
    outgate_weight,
    forget_floor,
    head_gain,
    output_weight,
    second_gain,
    second_gate,
    second_up,
    second_down,
):
    own_index = lax.axis_index(KV_TP)
    group_size = lax.axis_size(KV_TP)
    share_cols = tokens.shape[1]
    full_width = share_cols * group_size
    first_totals = fold_step(
        first_gain, first_gate, first_up, whole_of(tokens, (("kv_0", "kv_1"), "tp"), 1)
    )
    first_terms = channel_terms(tokens, first_totals, first_down, own_index, full_width)
    mixer_share = sum_in_two_steps(first_terms, (("kv_0", "kv_1"), "tp"), 1).astype(jnp.bfloat16)
    widened = mixer_share.astype(jnp.float32)
    squares = of_everyone(jnp.sum(widened * widened, axis=1), KV_TP)
    share_wide = mixer_share.astype(jnp.float32)
    mix_scaled = (
        share_wide * lax.dynamic_slice_in_dim(mix_gain, own_index * share_cols, share_cols)
    ).astype(jnp.bfloat16)
    state_rows, head_count, key_size, value_size = carried_state.shape
    projected = sum_by_axis(
        jnp.concatenate(
            [
                jnp.dot(mix_scaled, weight_part, preferred_element_type=jnp.float32)
                for weight_part in (query_weight, forget_weight, input_weight, outgate_weight)
            ],
            axis=1,
        ).astype(jnp.bfloat16),
        (("kv_0", "kv_1"), "tp"),
        0,
    )
    own_squares = lax.dynamic_slice_in_dim(squares, own_index * state_rows, state_rows)
    projected = projected * lax.rsqrt(own_squares / full_width + epsilon)[:, None]
    key_width = head_count * key_size
    value_width = head_count * value_size
    query_act = projected[:, :key_width].reshape(state_rows, head_count, key_size)
    forget_pre = projected[:, key_width : 2 * key_width].reshape(state_rows, head_count, key_size)
    input_val = projected[:, 2 * key_width : 2 * key_width + value_width].reshape(
        state_rows, head_count, value_size
    )
    gate_pre = projected[:, 2 * key_width + value_width :].reshape(
        state_rows, head_count, value_size
    )
    floor_grid = forget_floor.reshape(head_count, key_size)
    forget = floor_grid + (1.0 - floor_grid) * jax.nn.sigmoid(forget_pre)
    next_state = (
        forget[..., None] * carried_state + (1.0 - forget)[..., None] * input_val[:, :, None, :]
    )
    readout = jnp.sum(next_state * jax.nn.silu(query_act)[..., None], axis=2)
    normed = (
        readout
        * lax.rsqrt(jnp.mean(readout * readout, axis=-1, keepdims=True) + epsilon)
        * head_gain
    )
    mixer_out = (
        (normed * jax.nn.silu(gate_pre)).reshape(state_rows, value_width).astype(jnp.bfloat16)
    )
    update = jnp.dot(
        collect(mixer_out, KV_TP, 0), output_weight, preferred_element_type=jnp.float32
    )
    middle = (share_wide + update).astype(jnp.bfloat16)
    second_totals = fold_step(
        second_gain, second_gate, second_up, whole_of(middle, (("kv_0", "kv_1"), "tp"), 1)
    )
    second_terms = channel_terms(middle, second_totals, second_down, own_index, full_width)
    layer_out = sum_by_axis(second_terms.astype(jnp.bfloat16), (("kv_0", "kv_1"), "tp"), 1).astype(
        jnp.bfloat16
    )
    return (layer_out, next_state)


def solution(mesh):
    split = Mesh(
        mesh.devices.reshape(mesh.shape["dp"], 4, 4, mesh.shape["tp"]), ("dp", "kv_0", "kv_1", "tp")
    )
    return jax.shard_map(
        per_device,
        mesh=split,
        in_specs=(
            P("dp", KV_TP),
            P(DP_KV_TP, None, None, None),
            P(),
            P(None, KV_TP),
            P(None, KV_TP),
            P(KV_TP, None),
            P(),
            P(KV_TP, None),
            P(KV_TP, None),
            P(KV_TP, None),
            P(KV_TP, None),
            P(),
            P(),
            P(None, KV_TP),
            P(),
            P(None, KV_TP),
            P(None, KV_TP),
            P(KV_TP, None),
        ),
        out_specs=(P("dp", KV_TP), P(DP_KV_TP, None, None, None)),
        check_vma=False,
    )
```

profile of v0, /device:TPU:0, one launch (start us, length us, event | category | flops | bytes accessed | tf_op | source)
XLA Modules:
  0.0 309.2 jit_solution(16182927830919644007)
XLA Ops:
  0.6 2.2 broadcast_in_dim.12
  2.8 8.2 %all-to-all-start = ((bf16[16,256,128]{2,1,0:T(8,128)(2,1)}), bf16[16,256,128]{2,1,0:T(8,128)(2,1)}, u32[]{:S(2)}, u32[]{:S(2)}) async-start(bf16[16,256,128]{2,1,0:T(8,128)(2,1)} %broadcast_in_dim.12), calls=%async_computation | async-start | bytes 2097152 | tf_op jit(solution)/shard_map/all_to_all | solution.py:16
  11.0 17.7 %all-to-all-done = bf16[16,256,128]{2,1,0:T(8,128)(2,1)} async-done(((bf16[16,256,128]{2,1,0:T(8,128)(2,1)}), bf16[16,256,128]{2,1,0:T(8,128)(2,1)}, u32[]{:S(2)}, u32[]{:S(2)}) %all-to-all-start) | async-done | bytes 1048608 | tf_op jit(solution)/shard_map/all_to_all | solution.py:16
  28.8 1.7 broadcast_in_dim.13
  30.4 5.4 %all_to_all.61 = bf16[2,16,256,128]{3,2,1,0:T(8,128)(2,1)S(1)} all-to-all(bf16[2,16,256,128]{3,2,1,0:T(8,128)(2,1)S(1)} %broadcast_in_dim.13), channel_id=1, replica_groups=mesh['dp'=4,'kv_0'=4,'kv_1'=4,'tp'=2] {'tp'}, dimensions={0} | all-to-all | bytes 4194304 | tf_op jit(solution)/shard_map/all_to_all | solution.py:16
  35.9 0.5 multiply_reduce_fusion.2
  36.4 2.5 copy_convert_fusion.1
  38.9 5.6 %copy.101 = f32[256,32,128]{0,2,1:T(8,128)} copy(f32[256,32,128]{2,0,1:T(8,128)} %bitcast.81) | data formatting | bytes 8388608 | tf_op jit(solution)/shard_map/convert_element_type | solution.py:75
  44.5 2.7 fusion.1
  47.2 1.3 copy-done.2
  48.6 0.9 convolution_multiply_fusion.5
  49.5 8.1 %convolution_multiply_fusion.1 = f32[256,4096]{1,0:T(8,128)} fusion(bf16[352,4096]{1,0:T(8,128)(2,1)S(1)} %copy-done, bf16[4096,352]{0,1:T(8,128)(2,1)} %param.22, bf16[256,4096]{0,1:T(8,128)(2,1)} %copy-done.2, f32[256,352]{0,1:T(8,128)S(1)} %convolution_multiply_fusion.5, f32[256]{0:T(256)S(1)} %add_rsqrt_fusion.2), kind=kOutput, calls=%fused_computation.3 | convolution fusion | flops 1478074368 | bytes 12420096 | tf_op jit(solution)/shard_map/dot_general | solution.py:87
  57.7 1.6 add_dynamic-update-slice_fusion.1
  59.2 5.6 %copy.123 = f32[256,4096]{0,1:T(8,128)} copy(f32[256,4096]{1,0:T(8,128)} %add_dynamic-update-slice_fusion.1) | data formatting | bytes 8388608 | tf_op jit(solution)/shard_map/reshape | solution.py:35
  64.8 5.5 %copy.103 = f32[2,16,256,128]{3,1,2,0:T(8,128)} copy(f32[2,16,256,128]{2,3,0,1:T(8,128)} %bitcast.82) | data formatting | bytes 8388608 | tf_op jit(solution)/shard_map/transpose | solution.py:35
  70.3 11.9 %all_to_all.62 = f32[2,16,256,128]{3,1,2,0:T(8,128)} all-to-all(f32[2,16,256,128]{3,1,2,0:T(8,128)} %copy.103), channel_id=1, replica_groups=mesh['dp'=4,'kv_0'=4,'kv_1'=4,'tp'=2] {'tp'}, dimensions={0} | all-to-all | bytes 8388608 | tf_op jit(solution)/shard_map/all_to_all | solution.py:40
  82.2 2.7 reduce_sum.118
  84.9 2.0 copy.105
  86.9 3.9 %all-to-all-start.3 = ((f32[16,256,128]{2,1,0:T(8,128)}), f32[16,256,128]{2,1,0:T(8,128)S(1)}, u32[]{:S(2)}, u32[]{:S(2)}) async-start(f32[16,256,128]{2,1,0:T(8,128)} %copy.105), calls=%async_computation.3 | async-start | bytes 4194304 | tf_op jit(solution)/shard_map/all_to_all | solution.py:47
  90.8 0.8 dynamic_slice.6
  91.6 33.0 %all-to-all-done.3 = f32[16,256,128]{2,1,0:T(8,128)S(1)} async-done(((f32[16,256,128]{2,1,0:T(8,128)}), f32[16,256,128]{2,1,0:T(8,128)S(1)}, u32[]{:S(2)}, u32[]{:S(2)}) %all-to-all-start.3) | async-done | bytes 2097184 | tf_op jit(solution)/shard_map/all_to_all | solution.py:47
  124.6 0.1 reduce_sum.119
  124.7 0.1 fusion.23
  124.9 0.4 convolution_convert_fusion.1
  125.3 0.4 convolution_convert_fusion
  125.8 0.4 convolution_convert_fusion.3
  126.2 0.4 convolution_convert_fusion.2
  126.6 0.4 copy_bitcast_fusion
  127.1 8.2 %all_to_all.63 = bf16[2,16,8,8192]{3,2,1,0:T(8,128)(2,1)} all-to-all(bf16[2,16,8,8192]{3,2,1,0:T(8,128)(2,1)S(1)} %copy_bitcast_fusion), channel_id=1, replica_groups=mesh['dp'=4,'kv_0'=4,'kv_1'=4,'tp'=2] {'tp'}, dimensions={0} | all-to-all | bytes 8388608 | tf_op jit(solution)/shard_map/all_to_all | solution.py:56
  135.2 0.6 broadcast_in_dim.14
  135.9 4.2 %all-to-all-start.6 = ((f32[32,1,256]{2,1,0:T(1,128)}), f32[32,1,256]{2,1,0:T(1,128)S(1)}, u32[]{:S(2)}, u32[]{:S(2)}) async-start(f32[32,1,256]{2,1,0:T(1,128)} %broadcast_in_dim.14), calls=%async_computation.6 | async-start | bytes 65536 | tf_op jit(solution)/shard_map/all_to_all | solution.py:16
  140.0 5.0 %reduce_sum.120 = bf16[16,8,8192]{2,1,0:T(8,128)(2,1)} reduce(bf16[2,16,8,8192]{3,2,1,0:T(8,128)(2,1)} %all_to_all.63, bf16[]{:T(256)} %constant.51.clone.1), dimensions={0}, to_apply=%region_3.4 | reduce | flops 1048576 | bytes 6291458 | tf_op jit(solution)/shard_map/reduce_sum | solution.py:57
  145.0 2.3 all-to-all-done.6
  147.3 4.8 %all-to-all-start.5 = ((bf16[16,8,8192]{2,1,0:T(8,128)(2,1)}), bf16[16,8,8192]{2,1,0:T(8,128)(2,1)S(1)}, u32[]{:S(2)}, u32[]{:S(2)}) async-start(bf16[16,8,8192]{2,1,0:T(8,128)(2,1)} %reduce_sum.120), calls=%async_computation.5 | async-start | bytes 4194304 | tf_op jit(solution)/shard_map/all_to_all | solution.py:64
  152.2 0.1 add_rsqrt_fusion.3
  152.2 32.7 %all-to-all-done.5 = bf16[16,8,8192]{2,1,0:T(8,128)(2,1)S(1)} async-done(((bf16[16,8,8192]{2,1,0:T(8,128)(2,1)}), bf16[16,8,8192]{2,1,0:T(8,128)(2,1)S(1)}, u32[]{:S(2)}, u32[]{:S(2)}) %all-to-all-start.5) | async-done | bytes 2097184 | tf_op jit(solution)/shard_map/all_to_all | solution.py:64
  184.9 0.3 convert_reduce_fusion
  185.2 0.1 broadcast_multiply_fusion
  185.5 9.9 %multiply_reduce_fusion = (f32[8,16,128]{2,1,0:T(8,128)S(1)}, f32[8,16,128,128]{3,2,1,0:T(8,128)}) fusion(f32[8,16,128]{2,1,0:T(8,128)S(1)} %copy.114, f32[8,16,128]{2,1,0:T(8,128)S(1)} %copy.113, f32[8,16,128]{2,1,0:T(8,128)S(1)} %copy.112, f32[8,16,128,128]{3,2,1,0:T(8,128)} %param.19, f32[8,16,128]{2,1,0:T(8,128)S(1)} %copy.111), kind=kLoop, calls=%fused_computation | loop fusion | flops 10469376 | bytes 17104896 | tf_op jit(solution)/shard_map/reduce_sum | solution.py:158
  195.4 0.1 multiply_reduce_fusion.3
  195.5 0.1 multiply_bitcast_fusion
  195.6 0.1 broadcast_in_dim.15
  195.7 20.9 %all_to_all.64 = bf16[32,8,2048]{2,1,0:T(8,128)(2,1)S(1)} all-to-all(bf16[32,8,2048]{2,1,0:T(8,128)(2,1)S(1)} %broadcast_in_dim.15), channel_id=1, replica_groups=mesh['dp'=4,'kv_0'=4,'kv_1'=4,'tp'=2] {'kv_0','kv_1','tp'}, dimensions={0} | all-to-all | bytes 2097152 | tf_op jit(solution)/shard_map/all_to_all | solution.py:16
  216.7 0.4 fusion.6
  217.1 0.2 broadcast_in_dim.16
  217.3 20.9 %all_to_all.65 = bf16[16,256,128]{2,1,0:T(8,128)(2,1)S(1)} all-to-all(bf16[16,256,128]{2,1,0:T(8,128)(2,1)S(1)} %broadcast_in_dim.16), channel_id=1, replica_groups=mesh['dp'=4,'kv_0'=4,'kv_1'=4,'tp'=2] {'kv_0','kv_1'}, dimensions={0} | all-to-all | bytes 2097152 | tf_op jit(solution)/shard_map/all_to_all | solution.py:16
  238.2 0.5 broadcast_in_dim.17
  238.7 5.4 %all_to_all.66 = bf16[2,16,256,128]{3,2,1,0:T(8,128)(2,1)S(1)} all-to-all(bf16[2,16,256,128]{3,2,1,0:T(8,128)(2,1)S(1)} %broadcast_in_dim.17), channel_id=1, replica_groups=mesh['dp'=4,'kv_0'=4,'kv_1'=4,'tp'=2] {'tp'}, dimensions={0} | all-to-all | bytes 4194304 | tf_op jit(solution)/shard_map/all_to_all | solution.py:16
  244.1 0.5 multiply_reduce_fusion.1
  244.6 2.4 copy_convert_fusion
  247.0 5.6 %copy.117 = f32[256,32,128]{0,2,1:T(8,128)} copy(f32[256,32,128]{2,0,1:T(8,128)} %bitcast.83) | data formatting | bytes 8388608 | tf_op jit(solution)/shard_map/convert_element_type | solution.py:75
  252.7 2.7 fusion
  255.4 0.3 copy-done.14
  255.7 0.9 convolution_multiply_fusion.3
  256.7 8.2 %convolution_multiply_fusion = f32[256,4096]{1,0:T(8,128)} fusion(bf16[352,4096]{1,0:T(8,128)(2,1)} %param.35, bf16[4096,352]{0,1:T(8,128)(2,1)} %param.34, bf16[256,4096]{0,1:T(8,128)(2,1)S(1)} %fusion, f32[256,352]{0,1:T(8,128)S(1)} %convolution_multiply_fusion.3, f32[256]{0:T(256)S(1)} %add_rsqrt_fusion.1), kind=kOutput, calls=%fused_computation.2 | convolution fusion | flops 1478074368 | bytes 12420096 | tf_op jit(solution)/shard_map/dot_general | solution.py:87
  264.9 1.6 add_dynamic-update-slice_fusion
  266.5 2.5 convert_element_type.114
  269.0 2.5 copy.125
  271.5 3.5 %copy.119 = bf16[2,16,256,128]{3,1,2,0:T(8,128)(2,1)S(1)} copy(bf16[2,16,256,128]{2,3,0,1:T(8,128)(2,1)} %bitcast.84) | data formatting | bytes 4194304 | tf_op jit(solution)/shard_map/transpose | solution.py:35
  274.9 6.3 %all_to_all.67 = bf16[2,16,256,128]{3,1,2,0:T(8,128)(2,1)} all-to-all(bf16[2,16,256,128]{3,1,2,0:T(8,128)(2,1)S(1)} %copy.119), channel_id=1, replica_groups=mesh['dp'=4,'kv_0'=4,'kv_1'=4,'tp'=2] {'tp'}, dimensions={0} | all-to-all | bytes 4194304 | tf_op jit(solution)/shard_map/all_to_all | solution.py:56
  281.2 3.4 %reduce_sum.127 = bf16[16,256,128]{2,0,1:T(8,128)(2,1)} reduce(bf16[2,16,256,128]{3,1,2,0:T(8,128)(2,1)} %all_to_all.67, bf16[]{:T(256)} %constant.51.clone.1), dimensions={0}, to_apply=%region_10.11 | reduce | flops 524288 | bytes 3145730 | tf_op jit(solution)/shard_map/reduce_sum | solution.py:57
  284.7 1.5 copy.121
  286.1 21.1 %all_to_all.68 = bf16[16,256,128]{2,1,0:T(8,128)(2,1)} all-to-all(bf16[16,256,128]{2,1,0:T(8,128)(2,1)S(1)} %copy.121), channel_id=1, replica_groups=mesh['dp'=4,'kv_0'=4,'kv_1'=4,'tp'=2] {'kv_0','kv_1'}, dimensions={0} | all-to-all | bytes 2097152 | tf_op jit(solution)/shard_map/all_to_all | solution.py:64
  307.2 2.0 reduce_sum.128
  (41 shorter events, 0.3 us)
Async XLA Ops:
  0.6 48.9 %copy-start = (bf16[352,4096]{1,0:T(8,128)(2,1)S(1)}, bf16[352,4096]{1,0:T(8,128)(2,1)}, u32[]{:S(2)}) copy-start(bf16[352,4096]{1,0:T(8,128)(2,1)} %param.23) | copy-start | bytes 8650756
  2.8 25.9 %all-to-all-start = ((bf16[16,256,128]{2,1,0:T(8,128)(2,1)}), bf16[16,256,128]{2,1,0:T(8,128)(2,1)}, u32[]{:S(2)}, u32[]{:S(2)}) async-start(bf16[16,256,128]{2,1,0:T(8,128)(2,1)} %broadcast_in_dim.12), calls=%async_computation | async-start | bytes 2097152 | tf_op jit(solution)/shard_map/all_to_all | solution.py:16
  38.9 5.6 %copy-start.10 = (f32[4096]{0:T(1024)S(1)}, f32[4096]{0:T(1024)}, u32[]{:S(2)}) copy-start(f32[4096]{0:T(1024)} %param.20) | copy-start | bytes 49156
  44.5 4.1 %copy-start.13 = (bf16[4096,352]{0,1:T(8,128)(2,1)S(1)}, bf16[4096,352]{0,1:T(8,128)(2,1)}, u32[]{:S(2)}) copy-start(bf16[4096,352]{0,1:T(8,128)(2,1)} %param.21) | copy-start | bytes 8650756
  47.2 1.4 copy-start.2
  49.5 8.1 %copy-start.8 = (bf16[256,128]{1,0:T(8,128)(2,1)S(1)}, bf16[256,128]{1,0:T(8,128)(2,1)}, u32[]{:S(2)}) copy-start(bf16[256,128]{1,0:T(8,128)(2,1)} %param.18) | copy-start | bytes 196612
  86.9 37.9 %copy-start.3 = (bf16[128,2048]{1,0:T(8,128)(2,1)S(1)}, bf16[128,2048]{1,0:T(8,128)(2,1)}, u32[]{:S(2)}) copy-start(bf16[128,2048]{1,0:T(8,128)(2,1)} %param.27) | copy-start | bytes 1572868
  86.9 37.7 %all-to-all-start.3 = ((f32[16,256,128]{2,1,0:T(8,128)}), f32[16,256,128]{2,1,0:T(8,128)S(1)}, u32[]{:S(2)}, u32[]{:S(2)}) async-start(f32[16,256,128]{2,1,0:T(8,128)} %copy.105), calls=%async_computation.3 | async-start | bytes 4194304 | tf_op jit(solution)/shard_map/all_to_all | solution.py:47
  90.8 34.5 %copy-start.4 = (bf16[128,2048]{1,0:T(8,128)(2,1)S(1)}, bf16[128,2048]{1,0:T(8,128)(2,1)}, u32[]{:S(2)}) copy-start(bf16[128,2048]{1,0:T(8,128)(2,1)} %param.28) | copy-start | bytes 1572868
  124.7 1.0 copy-start.5
  124.7 1.5 copy-start.6
  135.9 11.4 %all-to-all-start.6 = ((f32[32,1,256]{2,1,0:T(1,128)}), f32[32,1,256]{2,1,0:T(1,128)S(1)}, u32[]{:S(2)}, u32[]{:S(2)}) async-start(f32[32,1,256]{2,1,0:T(1,128)} %broadcast_in_dim.14), calls=%async_computation.6 | async-start | bytes 65536 | tf_op jit(solution)/shard_map/all_to_all | solution.py:16
  145.0 7.1 %copy-start.12 = (f32[128]{0:T(128)S(1)}, f32[128]{0:T(128)}, u32[]{:S(2)}) copy-start(f32[128]{0:T(128)} %param.30) | copy-start | bytes 1540
  145.0 7.1 %copy-start.9 = (f32[2048]{0:T(1024)S(1)}, f32[2048]{0:T(1024)}, u32[]{:S(2)}) copy-start(f32[2048]{0:T(1024)} %param.29) | copy-start | bytes 24580
  147.3 37.7 %all-to-all-start.5 = ((bf16[16,8,8192]{2,1,0:T(8,128)(2,1)}), bf16[16,8,8192]{2,1,0:T(8,128)(2,1)S(1)}, u32[]{:S(2)}, u32[]{:S(2)}) async-start(bf16[16,8,8192]{2,1,0:T(8,128)(2,1)} %reduce_sum.120), calls=%async_computation.5 | async-start | bytes 4194304 | tf_op jit(solution)/shard_map/all_to_all | solution.py:64
  195.4 21.3 %copy-start.7 = (bf16[2048,128]{1,0:T(8,128)(2,1)S(1)}, bf16[2048,128]{1,0:T(8,128)(2,1)}, u32[]{:S(2)}) copy-start(bf16[2048,128]{1,0:T(8,128)(2,1)} %param.31) | copy-start | bytes 1572868
  247.0 5.6 %copy-start.11 = (f32[4096]{0:T(1024)S(1)}, f32[4096]{0:T(1024)}, u32[]{:S(2)}) copy-start(f32[4096]{0:T(1024)} %param.32) | copy-start | bytes 49156
  252.7 3.1 copy-start.14
  281.2 28.0 %copy-start.1 = (bf16[352,4096]{1,0:T(8,128)(2,1)S(1)}, bf16[352,4096]{1,0:T(8,128)(2,1)}, u32[]{:S(2)}) copy-start(bf16[352,4096]{1,0:T(8,128)(2,1)} %param.23) | copy-start | bytes 8650756
where the time goes:
time: 311 us; the launch traced here: 309 us
  blocking collectives  100 us (32%)
  waiting for transfers between devices  85.7 us (28%)
  other arithmetic  41.5 us (13%)
  local copies, waits for them, and re-layouts  39.6 us (13%)
  starting transfers between devices  21 us (7%)
  matrix products  20.3 us (7%)
    all_to_all x4, blocking collectives, copy_for_each(): lax.all_to_all(jnp.broadcast_to(shard[None], (devices, *shard.shape)), ax...  52.7 us
    all_to_all x1, waiting for transfers between devices, sum_in_two_steps(): return jnp.sum(lax.all_to_all(own, far, 0, 0, tiled=True), axis=0)  33 us
    all_to_all x1, waiting for transfers between devices, sum_by_axis(): lax.all_to_all(nearer.astype(jnp.bfloat16), far, split_axis=0, concat_axi...  32.7 us
    all_to_all x1, blocking collectives, sum_by_axis(): lax.all_to_all(nearer.astype(jnp.bfloat16), far, split_axis=0, concat_axi...  21.1 us
    all_to_all x2, waiting for transfers between devices, copy_for_each(): lax.all_to_all(jnp.broadcast_to(shard[None], (devices, *shard.shape)), ax...  20 us
    dot_general x2, matrix products, channel_terms(): jnp.dot(hidden, down_weight, preferred_element_type=jnp.float32)  16.4 us
    all_to_all x2, blocking collectives, sent_and_summed(): lax.all_to_all(in_blocks(shard, dim, devices), axis, 0, 0, tiled=True)  14.5 us
    all_to_all x2, starting transfers between devices, copy_for_each(): lax.all_to_all(jnp.broadcast_to(shard[None], (devices, *shard.shape)), ax...  12.4 us
  transfers between devices with their start and end apart: 4, of which 4 were waited for; matrix products, arithmetic and copies ran while one was open for 2% of the time, Pallas kernels for 0%

commit v1 on v0

v1 whole, which is shorter than its diff:
```python
import jax
import jax.numpy as jnp
from jax import lax
from jax.experimental import pallas as pl
from jax.experimental.pallas import tpu as pltpu
from jax.sharding import Mesh
from jax.sharding import PartitionSpec as P

KV_TP = ("kv_0", "kv_1", "tp")
DP_KV_TP = ("dp", "kv_0", "kv_1", "tp")
MESH = pl.DeviceIdType.MESH
HBM = pltpu.MemorySpace.HBM
VMEM = pltpu.MemorySpace.VMEM
F32 = jnp.float32
BF16 = jnp.bfloat16

epsilon = 1e-06
RING = 4
LANES = 128
CHIPS = RING * RING
BLOCKS = 2 * CHIPS
NEAR = (("kv_0", 1), ("kv_0", 3), ("kv_1", 1), ("kv_1", 3), ("tp", 1))
HALF_AXES = (("kv_1", "kv_0"), ("kv_0", "kv_1"))
FAR_FIRST = (2, 1, 3, 0)
CHIP_ORDER = tuple((a, b) for a in FAR_FIRST for b in FAR_FIRST if a == 2 or b == 2) + tuple(
    (a, b) for a in FAR_FIRST for b in FAR_FIRST if a != 2 and b != 2
)
POSITION = {chip: place for place, chip in enumerate(CHIP_ORDER)}


def own_place():
    return (lax.axis_index("kv_0"), lax.axis_index("kv_1"), lax.axis_index("tp"))


def block_of(place, along_0, along_1, other_core):
    at_0, at_1, core = place
    return (
        lax.rem(at_0 + along_0, RING) * (2 * RING)
        + lax.rem(at_1 + along_1, RING) * 2
        + lax.rem(core + other_core, 2)
    )


class Wire:
    def __init__(self, place, send_sems, recv_sems):
        at_0, at_1, core = place
        self.place = {"kv_0": (at_0, RING), "kv_1": (at_1, RING), "tp": (core, 2)}
        self.send_sems, self.recv_sems = send_sems, recv_sems
        self.used = 0
        self.sent = []

    def near(self, axis, step):
        at, size = self.place[axis]
        return {axis: lax.rem(at + step, size)}

    def greet(self):
        barrier = pltpu.get_barrier_semaphore()
        for axis, step in NEAR:
            pl.semaphore_signal(
                barrier, inc=1, device_id=self.near(axis, step), device_id_type=MESH
            )
        pl.semaphore_wait(barrier, len(NEAR))

    def take(self, count):
        first = self.used
        self.used += count
        return first

    def make(self, source, target, axis, step, slot):
        return pltpu.make_async_remote_copy(
            src_ref=source,
            dst_ref=target,
            send_sem=self.send_sems.at[slot],
            recv_sem=self.recv_sems.at[slot],
            device_id=self.near(axis, step),
            device_id_type=MESH,
        )

    def send(self, source, target, axis, step):
        copy = self.make(source, target, axis, step, self.take(1))
        copy.start()
        self.sent.append(copy)
        return copy

    def finish(self):
        for copy in self.sent:
            copy.wait_send()
        self.sent = []


def halves_of(rows):
    tiles = rows // 16
    first = (tiles - tiles // 2) * 16
    second = rows - first
    return ((0, first, first // 32 * 16), (first, second, second // 32 * 16))


def gather(wire, held):
    halves = halves_of(held.shape[3])
    copies = {}

    def view(half, first, second, part, slot=0):
        start, rows, cut = halves[half]
        start, rows = ((start, rows), (start, cut), (start + cut, rows - cut))[part]
        along = (second, first) if HALF_AXES[half][0] == "kv_1" else (first, second)
        return held.at[along[0], along[1], slot, pl.ds(start, rows), :]

    def spread(half, stage, first):
        for step, there in ((1, 3), (3, 1)):
            if stage == 0:
                source, target = view(half, 0, 0, 0), view(half, there, 0, 0)
            else:
                source, target = view(half, first, 0, 0), view(half, first, there, 0)
            copies[half, stage, first, there] = wire.send(
                source, target, HALF_AXES[half][stage], step
            )

    def relay(half, stage, first, came):
        copies[half, stage, first, came].wait_recv()
        step, part = (1, 1) if came == 3 else (3, 2)
        if stage == 0:
            source, target = view(half, came, 0, part), view(half, 2, 0, part)
        else:
            source, target = view(half, first, came, part), view(half, first, 2, part)
        copies[half, stage, first, 2, part] = wire.send(
            source, target, HALF_AXES[half][stage], step
        )

    def across(half, first, second):
        copies[half, "across", first, second] = wire.send(
            view(half, first, second, 0), view(half, first, second, 0, 1), "tp", 1
        )

    def far(half, stage, first):
        for part in (1, 2):
            copies[half, stage, first, 2, part].wait_recv()

    both = (0, 1)
    for half in both:
        spread(half, 0, 0)
    for half in both:
        spread(half, 1, 0)
    for half in both:
        across(half, 0, 0)
    for came in (3, 1):
        for half in both:
            relay(half, 0, 0, came)
            spread(half, 1, came)
            across(half, came, 0)
    for came in (3, 1):
        for half in both:
            relay(half, 1, 0, came)
            across(half, 0, came)
    for half in both:
        far(half, 0, 0)
        spread(half, 1, 2)
        across(half, 2, 0)
    for first in (3, 1):
        for came in (3, 1):
            for half in both:
                relay(half, 1, first, came)
                across(half, first, came)
    for half in both:
        far(half, 1, 0)
        across(half, 0, 2)
    for came in (3, 1):
        for half in both:
            relay(half, 1, 2, came)
            across(half, 2, came)
    for first in (3, 1, 2):
        for half in both:
            far(half, 1, first)
            across(half, first, 2)
    for key, copy in copies.items():
        if key[1] == "across":
            copy.wait_recv()


def scatter_sum(wire, rows, term, buffers):
    halves = halves_of(rows)
    early_out, early_in, late_out, late_in, last_out, last_in = buffers
    copies = {}

    def chip(half, first, second):
        return (second, first) if HALF_AXES[half][0] == "kv_1" else (first, second)

    def parts(half):
        start, count, cut = halves[half]
        return ((0, cut, 1), (cut, count - cut, 3))

    for turn, second in enumerate(FAR_FIRST):
        for half in (0, 1):
            start, count, _ = halves[half]
            early_out[half, turn, pl.ds(0, count), :] = term(
                chip(half, 2, second), start, count
            ).astype(BF16)
            for at, length, step in parts(half):
                copies["early", half, turn, step] = wire.send(
                    early_out.at[half, turn, pl.ds(at, length), :],
                    early_in.at[half, turn, pl.ds(at, length), :],
                    HALF_AXES[half][0],
                    step,
                )
    for turn, second in enumerate(FAR_FIRST):
        for half in (0, 1):
            start, count, _ = halves[half]
            for way, (at, length, step) in enumerate(parts(half)):
                near = chip(half, step, second)
                copies["early", half, turn, step].wait_recv()
                rest_at, rest = (length, count - length) if at == 0 else (0, at)
                late_out[half, turn, way, pl.ds(at, length), :] = (
                    term(near, start + at, length)
                    + early_in[half, turn, pl.ds(at, length), :].astype(F32)
                ).astype(BF16)
                late_out[half, turn, way, pl.ds(rest_at, rest), :] = term(
                    near, start + rest_at, rest
                ).astype(BF16)
                copies["late", half, turn, step] = wire.send(
                    late_out.at[half, turn, way, pl.ds(0, count), :],
                    late_in.at[half, turn, way, pl.ds(0, count), :],
                    HALF_AXES[half][0],
                    step,
                )
    sums = [None, None]
    for turn, second in enumerate(FAR_FIRST):
        for half in (0, 1):
            start, count, cut = halves[half]
            value = term(chip(half, 0, second), start, count)
            for way, (_, _, step) in enumerate(parts(half)):
                copies["late", half, turn, step].wait_recv()
                value += late_in[half, turn, way, pl.ds(0, count), :].astype(F32)
            axis = HALF_AXES[half][1]
            if second == 2:
                last_out[half, 0, pl.ds(0, count), :] = value.astype(BF16)
                for at, length, step in parts(half):
                    copies["last", half, step] = wire.send(
                        last_out.at[half, 0, pl.ds(at, length), :],
                        last_in.at[half, 0, pl.ds(at, length), :],
                        axis,
                        step,
                    )
            elif second == 0:
                sums[half] = value
            else:
                way = 1 if second == 1 else 2
                at, length, step = parts(half)[way - 1]
                rest_at, rest = (length, count - length) if at == 0 else (0, at)
                copies["last", half, step].wait_recv()
                last_out[half, way, pl.ds(at, length), :] = (
                    value[at : at + length]
                    + last_in[half, 0, pl.ds(at, length), :].astype(F32)
                ).astype(BF16)
                last_out[half, way, pl.ds(rest_at, rest), :] = value[
                    rest_at : rest_at + rest
                ].astype(BF16)
                copies["final", half, step] = wire.send(
                    last_out.at[half, way, pl.ds(0, count), :],
                    last_in.at[half, way, pl.ds(0, count), :],
                    axis,
                    step,
                )
    for half in (0, 1):
        count = halves[half][1]
        for way, step in ((1, 1), (2, 3)):
            copies["final", half, step].wait_recv()
            sums[half] += last_in[half, way, pl.ds(0, count), :].astype(F32)
    return sums


def scatter_buffers(rows):
    half = halves_of(rows)[0][1]
    return [
        pltpu.VMEM((2, RING, half, LANES), BF16),
        pltpu.VMEM((2, RING, half, LANES), BF16),
        pltpu.VMEM((2, RING, 2, half, LANES), BF16),
        pltpu.VMEM((2, RING, 2, half, LANES), BF16),
        pltpu.VMEM((2, 3, half, LANES), BF16),
        pltpu.VMEM((2, 3, half, LANES), BF16),
    ]


def load_feed_forward(place, gate_hbm, up_hbm, down_hbm, wide, down, sems):
    hidden = gate_hbm.shape[0]
    half = wide.shape[0] // 2
    for block in range(BLOCKS):
        along_0, along_1, other = block // (2 * RING), block // 2 % RING, block % 2
        columns = pl.ds(
            pl.multiple_of(block_of(place, along_0, along_1, other) * LANES, LANES), LANES
        )
        here = pl.ds(block * LANES, LANES)
        pltpu.make_async_copy(
            gate_hbm.at[:, columns], wide.at[pl.ds(0, hidden), here], sems.at[0]
        ).start()
        pltpu.make_async_copy(
            up_hbm.at[:, columns], wide.at[pl.ds(half, hidden), here], sems.at[1]
        ).start()
    for at, (along_0, along_1) in enumerate(CHIP_ORDER):
        for other in (0, 1):
            columns = pl.ds(
                pl.multiple_of(block_of(place, along_0, along_1, other) * LANES, LANES), LANES
            )
            pltpu.make_async_copy(
                down_hbm.at[:, columns], down.at[at, :, pl.ds(other * LANES, LANES)], sems.at[2]
            ).start()
    return hidden, half


def feed_forward(
    place, wire, held, gain, gate_hbm, up_hbm, down_hbm, wide, down, sems, scratch, buffers
):
    scaled, squares, acc, own, pair_out, pair_in = scratch
    hidden, half = (gate_hbm.shape[0], wide.shape[0] // 2)
    rows = scaled.shape[0]
    width = scaled.shape[1]
    squares[...] = jnp.zeros_like(squares)

    def scale(block, carry):
        entry = held[block // (2 * RING), block // 2 % RING, block % 2].astype(F32)
        index = block_of(place, block // (2 * RING), block // 2 % RING, block % 2)
        squares[...] += entry * entry
        scaled[:, pl.ds(pl.multiple_of(block * LANES, LANES), LANES)] = (
            entry * gain[pl.ds(index, 1), :]
        ).astype(BF16)
        return carry

    lax.fori_loop(0, BLOCKS, scale, 0)
    pltpu.make_async_copy(gate_hbm, wide.at[pl.ds(0, hidden), :], sems.at[0]).wait()
    pltpu.make_async_copy(up_hbm, wide.at[pl.ds(half, hidden), :], sems.at[1]).wait()
    acc[...] = jnp.zeros_like(acc)
    depth = width // 4

    def product(step, carry):
        chunk = pl.ds(pl.multiple_of(step * depth, depth), depth)
        acc[...] += lax.dot_general(
            scaled[:, chunk],
            wide[:, chunk],
            (((1,), (1,)), ((), ())),
            preferred_element_type=F32,
        )
        return carry

    lax.fori_loop(0, 4, product, 0)
    row_scale = lax.rsqrt(jnp.sum(squares[...], axis=1, keepdims=True) / width + epsilon)
    gate = row_scale * acc[:, :hidden]
    up = row_scale * acc[:, half : half + hidden]
    units = (gate / (1.0 + jnp.exp(-gate)) * up).astype(BF16)
    pltpu.make_async_copy(down, down, sems.at[2]).wait()
    first = wire.take(CHIPS)

    def pair_copy(at):
        return wire.make(pair_out.at[at], pair_in.at[at], "tp", 1, first + at)

    def project(at, carry):
        result = jnp.dot(units, down[at], preferred_element_type=F32)
        own[at] = result[:, :LANES]
        pair_out[at] = result[:, LANES:].astype(BF16)
        pair_copy(at).start()
        return carry

    lax.fori_loop(0, CHIPS, project, 0)
    arrived = set()

    def term(chip, start, count):
        at = POSITION[chip]
        if at not in arrived:
            arrived.add(at)
            pair_copy(at).wait_recv()
        return own[at, pl.ds(start, count), :] + pair_in[at, pl.ds(start, count), :].astype(F32)

    sums = scatter_sum(wire, rows, term, buffers)
    wire.sent += [pair_copy(at) for at in range(CHIPS)]
    return sums


def feed_forward_scratch(rows, width, hidden):
    half = -(-hidden // LANES) * LANES
    return [
        pltpu.VMEM((RING, RING, 2, rows, LANES), BF16),
        pltpu.VMEM((2 * half, width), BF16),
        pltpu.VMEM((CHIPS, hidden, 2 * LANES), BF16),
        pltpu.SemaphoreType.DMA((8,)),
        pltpu.VMEM((rows, width), BF16),
        pltpu.VMEM((rows, LANES), F32),
        pltpu.VMEM((rows, 2 * half), F32),
        pltpu.VMEM((CHIPS, rows, LANES), F32),
        pltpu.VMEM((CHIPS, rows, LANES), BF16),
        pltpu.VMEM((CHIPS, rows, LANES), BF16),
        *scatter_buffers(rows),
    ]


def clear_padding(wide, hidden):
    half = wide.shape[0] // 2
    for start in (hidden, half + hidden):
        wide[pl.ds(start, half - hidden), :] = jnp.zeros((half - hidden, wide.shape[1]), BF16)


def first_kernel(
    tokens,
    gate_hbm,
    up_hbm,
    down_hbm,
    first_gain,
    mix_gain,
    query_hbm,
    forget_hbm,
    input_hbm,
    outgate_hbm,
    projected,
    mixer_share,
    send_sems,
    recv_sems,
    held,
    wide,
    down,
    sems,
    scaled,
    squares,
    acc,
    own,
    pair_out,
    pair_in,
    *rest,
):
    buffers, (low, high, share, ordered, wide_own, wide_out, wide_in), wide_buffers = (
        rest[:6],
        rest[6:13],
        rest[13:],
    )
    place = own_place()
    wire = Wire(place, send_sems, recv_sems)
    own_tokens = pltpu.make_async_copy(tokens, held.at[0, 0, 0], sems.at[3])
    own_tokens.start()
    wire.greet()
    own_tokens.wait()
    load_feed_forward(place, gate_hbm, up_hbm, down_hbm, wide, down, sems)
    width = query_hbm.shape[1]
    loads = [
        pltpu.make_async_copy(source, target.at[:, pl.ds(at, width)], sems.at[4 + index])
        for index, (source, target, at) in enumerate(
            (
                (query_hbm, low, 0),
                (forget_hbm, low, width),
                (input_hbm, high, 0),
                (outgate_hbm, high, width),
            )
        )
    ]
    for load in loads:
        load.start()
    clear_padding(wide, gate_hbm.shape[0])
    gather(wire, held)
    sums = feed_forward(
        place,
        wire,
        held,
        first_gain,
        gate_hbm,
        up_hbm,
        down_hbm,
        wide,
        down,
        sems,
        (scaled, squares, acc, own, pair_out, pair_in),
        buffers,
    )
    rows = share.shape[0]
    for (start, count, _), value in zip(halves_of(rows), sums):
        part = pl.ds(start, count)
        mixed = (held[0, 0, 0, part, :].astype(F32) + 0.5 * value).astype(BF16)
        mixer_share[part, :] = mixed
        share[part, :] = mixed.astype(F32)
    seqs = rows // BLOCKS
    for block in range(BLOCKS):
        index = block_of(place, block // (2 * RING), block // 2 % RING, block % 2)
        ordered[pl.ds(block * seqs, seqs), :] = share[
            pl.ds(pl.multiple_of(index * seqs, seqs), seqs), :
        ]
    entry = ordered[...]
    index = block_of(place, 0, 0, 0)
    mix_scaled = (entry * mix_gain[pl.ds(index, 1), :]).astype(BF16)
    square_sum = jnp.broadcast_to(jnp.sum(entry * entry, axis=1, keepdims=True), entry.shape)
    for load in loads:
        load.wait()

    def keep(at, lower, upper):
        pair = jnp.concatenate(
            [lower.reshape(BLOCKS, seqs, LANES), upper.reshape(BLOCKS, seqs, LANES)], axis=1
        ).reshape(CHIPS, 2, 2 * seqs, LANES)
        wide_own[:, pl.ds(at, 2 * seqs), :] = pair[:, 0]
        wide_out[:, pl.ds(at, 2 * seqs), :] = pair[:, 1].astype(BF16)

    columns = low.shape[1]
    tile = 2 * seqs

    def project(step, carry):
        chunk = pl.ds(pl.multiple_of(step * (2 * LANES), 2 * LANES), 2 * LANES)
        lower = jnp.dot(mix_scaled, low[:, chunk], preferred_element_type=F32)
        upper = jnp.dot(mix_scaled, high[:, chunk], preferred_element_type=F32)
        for which in (0, 1):
            at = pl.multiple_of(step * (2 * tile) + which * tile, tile)
            lanes = slice(which * LANES, (which + 1) * LANES)
            keep(at, lower[:, lanes], upper[:, lanes])
        return carry

    lax.fori_loop(0, columns // (2 * LANES), project, 0)
    keep(columns // LANES * tile, square_sum, jnp.zeros_like(square_sum))
    across = []
    wide_rows = wide_own.shape[1]
    for start, count, _ in halves_of(wide_rows):
        part = pl.ds(start, count)
        across.append(wire.send(wide_out.at[:, part, :], wide_in.at[:, part, :], "tp", 1))
    for copy in across:
        copy.wait_recv()

    def term(chip, start, count):
        at = chip[0] * RING + chip[1]
        part = pl.ds(start, count)
        return wide_own[at, part, :] + wide_in[at, part, :].astype(F32)

    sums = scatter_sum(wire, wide_rows, term, wide_buffers)
    for (start, count, _), value in zip(halves_of(wide_rows), sums):
        projected[pl.ds(start, count), :] = value
    wire.finish()


def state_kernel(
    full_width, projected, squares, floor_grid, head_gain, state, next_state, mixer_out
):
    head = pl.program_id(0)
    heads = pl.num_programs(0)
    seqs, _, keys, values = state.shape
    tile = 2 * seqs
    scale = lax.rsqrt(squares[...] / full_width + epsilon)

    def channels(block, second):
        return scale * projected[
            pl.ds(pl.multiple_of(block * tile + second * seqs, seqs), seqs), :
        ]

    query = channels(head, 0)
    entering = channels(head, 1)
    forget_pre = channels(heads + head, 0)
    gate = channels(heads + head, 1)
    floor = floor_grid[pl.ds(head, 1), :]
    forget = floor + (1.0 - floor) / (1.0 + jnp.exp(-forget_pre))
    query = query / (1.0 + jnp.exp(-query))
    forget_columns = forget.T
    query_columns = query.T
    readouts = []
    for seq in range(seqs):
        kept = jnp.broadcast_to(forget_columns[:, seq : seq + 1], (keys, values))
        asked = jnp.broadcast_to(query_columns[:, seq : seq + 1], (keys, values))
        after = kept * state[seq, 0] + (1.0 - kept) * entering[seq : seq + 1, :]
        next_state[seq, 0] = after
        readouts.append(jnp.sum(after * asked, axis=0, keepdims=True))
    readout = jnp.concatenate(readouts, axis=0)
    normed = (
        readout
        * lax.rsqrt(jnp.mean(readout * readout, axis=-1, keepdims=True) + epsilon)
        * head_gain[...]
    )
    half = heads // 2
    row = lax.rem(head, half) * tile + (head // half) * seqs
    mixer_out[pl.ds(pl.multiple_of(row, seqs), seqs), :] = normed * (gate / (1.0 + jnp.exp(-gate)))


def second_kernel(
    mixer_out,
    mixer_share,
    output_hbm,
    gate_hbm,
    up_hbm,
    down_hbm,
    second_gain,
    layer_out,
    send_sems,
    recv_sems,
    held,
    wide,
    down,
    sems,
    scaled,
    squares,
    acc,
    own,
    pair_out,
    pair_in,
    *rest,
):
    buffers, (mixed, output, update) = rest[:6], rest[6:]
    place = own_place()
    wire = Wire(place, send_sems, recv_sems)
    depth = output.shape[0]
    loads = [
        pltpu.make_async_copy(
            output_hbm.at[pl.ds(which * depth, depth), :],
            output.at[:, pl.ds(which * LANES, LANES)],
            sems.at[3 + which],
        )
        for which in (0, 1)
    ]
    for load in loads:
        load.start()
    mixed[0, 0, 0] = mixer_out[...].astype(BF16)
    wire.greet()
    load_feed_forward(place, gate_hbm, up_hbm, down_hbm, wide, down, sems)
    clear_padding(wide, gate_hbm.shape[0])
    gather(wire, mixed)
    for load in loads:
        load.wait()
    rows = update.shape[0]
    seqs = rows // BLOCKS
    tile = 2 * seqs
    total = None
    for step in range(depth // (2 * LANES)):
        pieces = [
            mixed[:, :, :, pl.ds((2 * step + which) * tile, tile), :].reshape(
                BLOCKS * tile, LANES
            )
            for which in (0, 1)
        ]
        product = jnp.dot(
            jnp.concatenate(pieces, axis=1),
            output[pl.ds(step * 2 * LANES, 2 * LANES), :],
            preferred_element_type=F32,
        )
        total = product if total is None else total + product
    total = total.reshape(BLOCKS, tile, 2 * LANES)
    total = total[:, :seqs, :LANES] + total[:, seqs:, LANES:]
    for block in range(BLOCKS):
        index = block_of(place, block // (2 * RING), block // 2 % RING, block % 2)
        update[pl.ds(pl.multiple_of(index * seqs, seqs), seqs), :] = total[block]
    held[0, 0, 0] = (mixer_share[...].astype(F32) + update[...]).astype(BF16)
    gather(wire, held)
    sums = feed_forward(
        place,
        wire,
        held,
        second_gain,
        gate_hbm,
        up_hbm,
        down_hbm,
        wide,
        down,
        sems,
        (scaled, squares, acc, own, pair_out, pair_in),
        buffers,
    )
    for (start, count, _), value in zip(halves_of(rows), sums):
        part = pl.ds(start, count)
        layer_out[part, :] = (held[0, 0, 0, part, :].astype(F32) + 0.5 * value).astype(BF16)
    wire.finish()


def in_space(*spaces):
    return [pl.BlockSpec(memory_space=space) for space in spaces]


def kernel_params(identity):
    return pltpu.CompilerParams(
        collective_id=identity, has_side_effects=True, vmem_limit_bytes=62 << 20
    )


def per_device(
    tokens,
    carried_state,
    first_gain,
    first_gate,
    first_up,
    first_down,
    mix_gain,
    query_weight,
    forget_weight,
    input_weight,
    outgate_weight,
    forget_floor,
    head_gain,
    output_weight,
    second_gain,
    second_gate,
    second_up,
    second_down,
):
    rows, share = tokens.shape
    full_width, hidden = first_gate.shape
    seqs, heads, keys, values = carried_state.shape
    tile = 2 * seqs
    wide_rows = (2 * heads + 1) * tile
    by_block = (full_width // LANES, LANES)
    projected, mixer_share = pl.pallas_call(
        first_kernel,
        name="first_block",
        out_shape=(
            jax.ShapeDtypeStruct((wide_rows, LANES), F32),
            jax.ShapeDtypeStruct((rows, share), BF16),
        ),
        in_specs=in_space(HBM, HBM, HBM, HBM, VMEM, VMEM, HBM, HBM, HBM, HBM),
        out_specs=in_space(VMEM, VMEM),
        scratch_shapes=[
            pltpu.SemaphoreType.DMA((192,)),
            pltpu.SemaphoreType.DMA((192,)),
            *feed_forward_scratch(rows, full_width, hidden),
            pltpu.VMEM((share, 2 * heads * keys), BF16),
            pltpu.VMEM((share, 2 * heads * values), BF16),
            pltpu.VMEM((rows, LANES), F32),
            pltpu.VMEM((rows, LANES), F32),
            pltpu.VMEM((CHIPS, wide_rows, LANES), F32),
            pltpu.VMEM((CHIPS, wide_rows, LANES), BF16),
            pltpu.VMEM((CHIPS, wide_rows, LANES), BF16),
            *scatter_buffers(wide_rows),
        ],
        compiler_params=kernel_params(0),
    )(
        tokens,
        first_gate.T,
        first_up.T,
        first_down,
        first_gain.reshape(by_block),
        mix_gain.reshape(by_block),
        query_weight,
        forget_weight,
        input_weight,
        outgate_weight,
    )
    whole = lambda *shape: pl.BlockSpec(shape, lambda head: (0,) * len(shape))
    one_head = pl.BlockSpec((seqs, 1, keys, values), lambda head: (0, head, 0, 0))
    next_state, mixer_out = pl.pallas_call(
        lambda *refs: state_kernel(full_width, *refs),
        name="state_update",
        grid=(heads,),
        out_shape=(
            jax.ShapeDtypeStruct(carried_state.shape, F32),
            jax.ShapeDtypeStruct((heads * seqs, values), F32),
        ),
        in_specs=[
            whole(wide_rows, LANES),
            pl.BlockSpec((seqs, LANES), lambda head: (2 * (wide_rows // tile - 1), 0)),
            whole(heads, keys),
            whole(1, values),
            one_head,
        ],
        out_specs=(one_head, whole(heads * seqs, values)),
        compiler_params=pltpu.CompilerParams(dimension_semantics=("arbitrary",)),
    )(
        projected,
        projected,
        forget_floor.reshape(heads, keys),
        head_gain.reshape(1, values),
        carried_state,
    )
    layer_out = pl.pallas_call(
        second_kernel,
        name="second_block",
        out_shape=jax.ShapeDtypeStruct((rows, share), BF16),
        in_specs=in_space(VMEM, VMEM, HBM, HBM, HBM, HBM, VMEM),
        out_specs=pl.BlockSpec(memory_space=VMEM),
        scratch_shapes=[
            pltpu.SemaphoreType.DMA((224,)),
            pltpu.SemaphoreType.DMA((224,)),
            *feed_forward_scratch(rows, full_width, hidden),
            pltpu.VMEM((RING, RING, 2, heads * seqs, LANES), BF16),
            pltpu.VMEM((heads * values // 2, 2 * LANES), BF16),
            pltpu.VMEM((rows, LANES), F32),
        ],
        compiler_params=kernel_params(1),
    )(
        mixer_out,
        mixer_share,
        output_weight,
        second_gate.T,
        second_up.T,
        second_down,
        second_gain.reshape(by_block),
    )
    return (layer_out, next_state)


def solution(mesh):
    split = Mesh(
        mesh.devices.reshape(mesh.shape["dp"], RING, RING, mesh.shape["tp"]), DP_KV_TP
    )
    return jax.shard_map(
        per_device,
        mesh=split,
        in_specs=(
            P("dp", KV_TP),
            P(DP_KV_TP, None, None, None),
            P(),
            P(None, KV_TP),
            P(None, KV_TP),
            P(KV_TP, None),
            P(),
            P(KV_TP, None),
            P(KV_TP, None),
            P(KV_TP, None),
            P(KV_TP, None),
            P(),
            P(),
            P(None, KV_TP),
            P(),
            P(None, KV_TP),
            P(None, KV_TP),
            P(KV_TP, None),
        ),
        out_specs=(P("dp", KV_TP), P(DP_KV_TP, None, None, None)),
        check_vma=False,
    )
```

time: 311 us -> 147 us (0.47)
  Pallas kernels: 0 us -> 145 us
  blocking collectives: 100 us -> 0 us
  waiting for transfers between devices: 85.7 us -> 0 us
  other arithmetic: 41.5 us -> 0 us
  local copies, waits for them, and re-layouts: 39.6 us -> 1.47 us
  starting transfers between devices: 21 us -> 0 us
  matrix products: 20.3 us -> 0 us
    pallas_call x0 -> x3, Pallas kernels: none -> 145 us  [the longest x1 70.1 us: per_device(): pl.pallas_call(first_kernel, name='first_block', out_shape=(jax.ShapeDtyp...]
    all_to_all x8 -> x0, blocking collectives: 100 us -> none  [the longest x4 52.7 us: copy_for_each(): lax.all_to_all(jnp.broadcast_to(shard[None], (devices, *shard.shape)), ax...]
    all_to_all x4 -> x0, waiting for transfers between devices: 85.7 us -> none  [the longest x1 33 us: sum_in_two_steps(): return jnp.sum(lax.all_to_all(own, far, 0, 0, tiled=True), axis=0)]
    reduce_sum x12 -> x0, other arithmetic: 24.6 us -> none  [the longest x1 9.89 us: per_device(): readout = jnp.sum(next_state * jax.nn.silu(query_act)[..., None], axis=2)]
    all_to_all x4 -> x0, starting transfers between devices: 21 us -> none  [the longest x2 12.4 us: copy_for_each(): lax.all_to_all(jnp.broadcast_to(shard[None], (devices, *shard.shape)), ax...]
    dot_general x9 -> x0, matrix products: 20.3 us -> none  [the longest x2 16.4 us: channel_terms(): jnp.dot(hidden, down_weight, preferred_element_type=jnp.float32)]
    convert_element_type x6 -> x0, other arithmetic: 12.9 us -> none  [the longest x2 5.46 us: fold_step(): scaled = (widened * gain_vec).astype(jnp.bfloat16)]
    convert_element_type x2 -> x0, local copies, waits for them, and re-layouts: 11.2 us -> none  [fold_step(): widened = block_cols.astype(jnp.float32)]
  transfers between devices with their start and end apart: 4 -> 0, of which waited for: 4 -> 0; matrix products, arithmetic and copies ran while one was open for 2% -> 0% of each run, Pallas kernels for 0% -> 0%
where the time goes in v1:
time: 147 us
  Pallas kernels  145 us (99%)
  local copies, waits for them, and re-layouts  1.47 us (1%)
    pallas_call x1, Pallas kernels, per_device(): pl.pallas_call(first_kernel, name='first_block', out_shape=(jax.ShapeDtyp...  70.1 us
    pallas_call x1, Pallas kernels, per_device(): pl.pallas_call(second_kernel, name='second_block', out_shape=jax.ShapeDty...  57.7 us
    pallas_call x1, Pallas kernels, per_device(): pl.pallas_call(lambda *refs: state_kernel(full_width, *refs), name='state...  16.9 us

profile of v1, /device:TPU:0, one launch (start us, length us, event | category | flops | bytes accessed | tf_op | source)
XLA Modules:
  0.0 146.8 jit_solution(17768375852144809171)
XLA Ops:
  0.6 70.1 %first_block.1 = (f32[528,128]{1,0:T(8,128)}, bf16[256,128]{1,0:T(8,128)(2,1)}) custom-call(bf16[256,128]{1,0:T(8,128)(2,1)} %tokens.1, bf16[352,4096]{1,0:T(8,128)(2,1)} %bitcast.9, bf16[352,4096]{1,0:T(8,128)(2,1)} %bitcast.10, bf16[352,4096]{1,0:T(8,128)(2,1)} %down_hbm.2, f32[32,128]{1,0:T(8,128)} %bitcast.13, f32[32,128]{1,0:T(8,128)} %bitcast.14, ...), custom_call_target="tpu_custom_call" | custom-call | tf_op jit(solution)/shard_map/first_block/pallas_call | solution.py:692
  70.7 16.9 %state_update.1 = (f32[8,16,128,128]{3,2,1,0:T(8,128)}, f32[128,128]{1,0:T(8,128)}) custom-call(f32[528,128]{1,0:T(8,128)} %get-tuple-element.6.refs_0_.refs_1_, f32[528,128]{1,0:T(8,128)} %get-tuple-element.6.refs_0_.refs_1_, f32[16,128]{1,0:T(8,128)} %bitcast.16, f32[1,128]{1,0:T(1,128)} %bitcast.17, f32[8,16,128,128]{3,2,1,0:T(8,128)} %refs_4_.1), custom_call_target="tpu_custom_call" | custom-call | tf_op jit(solution)/shard_map/state_update/pallas_call | solution.py:729
  87.6 57.7 %second_block.1 = bf16[256,128]{1,0:T(8,128)(2,1)} custom-call(f32[128,128]{1,0:T(8,128)} %get-tuple-element.7.mixer_out, bf16[256,128]{1,0:T(8,128)(2,1)} %get-tuple-element.8.mixer_share, bf16[2048,128]{1,0:T(8,128)(2,1)} %output_hbm.1, bf16[352,4096]{1,0:T(8,128)(2,1)} %bitcast.11, bf16[352,4096]{1,0:T(8,128)(2,1)} %bitcast.12, ...), custom_call_target="tpu_custom_call" | custom-call | tf_op jit(solution)/shard_map/second_block/pallas_call | solution.py:753
  145.3 1.5 %copy.21 = bf16[256,128]{1,0:T(8,128)(2,1)} copy(bf16[256,128]{1,0:T(8,128)(2,1)} %second_block.1) | data formatting | bytes 131072

commit v2 on v1

v2 whole, which is shorter than its diff:
```python
import jax
import jax.numpy as jnp
from jax import lax
from jax.experimental import pallas as pl
from jax.experimental.pallas import tpu as pltpu
from jax.sharding import Mesh
from jax.sharding import PartitionSpec as P

KV_TP = ("kv_0", "kv_1", "tp")
DP_KV_TP = ("dp", "kv_0", "kv_1", "tp")
MESH = pl.DeviceIdType.MESH
HBM = pltpu.MemorySpace.HBM
VMEM = pltpu.MemorySpace.VMEM
F32 = jnp.float32
BF16 = jnp.bfloat16

epsilon = 1e-06
RING = 4
LANES = 128
CHIPS = RING * RING
BLOCKS = 2 * CHIPS
NEAR = tuple((axis, step) for axis in ("kv_0", "kv_1") for step in (2, 1, 3)) + (("tp", 1),)
HALF_AXES = (("kv_1", "kv_0"), ("kv_0", "kv_1"))
FAR_FIRST = (2, 1, 3, 0)
NEAR_FIRST = (1, 3, 2)
STEPS = (2, 1, 3)
IN_LINE = ((0, 0),) + tuple((0, a) for a in NEAR_FIRST) + tuple((a, 0) for a in NEAR_FIRST)
ASIDE = tuple((a, b) for a in NEAR_FIRST for b in NEAR_FIRST)
GROUPS = (
    tuple((*chip, core) for core in (0, 1) for chip in IN_LINE),
    tuple((*chip, 0) for chip in ASIDE),
    tuple((*chip, 1) for chip in ASIDE),
)
ORDER = GROUPS[0] + GROUPS[1] + GROUPS[2]
KEPT_AT = {block: at for at, block in enumerate(ORDER)}
FIRST_CHIPS = tuple(
    chip
    for turn in FAR_FIRST
    for step in STEPS
    for chip in ((step, turn), (turn, step))
)
CHIP_ORDER = tuple(dict.fromkeys(FIRST_CHIPS)) + ((0, 0),)
POSITION = {chip: place for place, chip in enumerate(CHIP_ORDER)}


def own_place():
    return (lax.axis_index("kv_0"), lax.axis_index("kv_1"), lax.axis_index("tp"))


def block_of(place, along_0, along_1, other_core):
    at_0, at_1, core = place
    return (
        lax.rem(at_0 + along_0, RING) * (2 * RING)
        + lax.rem(at_1 + along_1, RING) * 2
        + lax.rem(core + other_core, 2)
    )


class Wire:
    def __init__(self, place, send_sems, recv_sems):
        at_0, at_1, core = place
        self.place = {"kv_0": (at_0, RING), "kv_1": (at_1, RING), "tp": (core, 2)}
        self.send_sems, self.recv_sems = send_sems, recv_sems
        self.used = 0
        self.sent = []

    def near(self, axis, step):
        at, size = self.place[axis]
        return {axis: lax.rem(at + step, size)}

    def greet(self):
        barrier = pltpu.get_barrier_semaphore()
        for axis, step in NEAR:
            pl.semaphore_signal(
                barrier, inc=1, device_id=self.near(axis, step), device_id_type=MESH
            )
        pl.semaphore_wait(barrier, len(NEAR))

    def take(self, count):
        first = self.used
        self.used += count
        return first

    def make(self, source, target, axis, step, slot):
        return pltpu.make_async_remote_copy(
            src_ref=source,
            dst_ref=target,
            send_sem=self.send_sems.at[slot],
            recv_sem=self.recv_sems.at[slot],
            device_id=self.near(axis, step),
            device_id_type=MESH,
        )

    def send(self, source, target, axis, step):
        copy = self.make(source, target, axis, step, self.take(1))
        copy.start()
        self.sent.append(copy)
        return copy

    def finish(self):
        for copy in self.sent:
            copy.wait_send()
        self.sent = []


def halves_of(rows):
    tiles = rows // 16
    first = (tiles - tiles // 2) * 16
    second = rows - first
    return ((0, first, first // 32 * 16), (first, second, second // 32 * 16))


def gather(wire, held, ready=None):
    halves = halves_of(held.shape[1])
    copies = {}

    def view(half, first, second, core=0):
        start, rows, _ = halves[half]
        along = (second, first) if HALF_AXES[half][0] == "kv_1" else (first, second)
        return held.at[KEPT_AT[(*along, core)], pl.ds(start, rows), :]

    def spread(half, stage, first, steps=STEPS):
        for step in steps:
            there = RING - step
            target = view(half, there, 0) if stage == 0 else view(half, first, there)
            copies[half, stage, first, there] = wire.send(
                view(half, first, 0), target, HALF_AXES[half][stage], step
            )

    def across(half, first, second):
        copies[half, "across", first, second] = wire.send(
            view(half, first, second), view(half, first, second, 1), "tp", 1
        )

    def arrive(half, stage, first, there):
        copies[half, stage, first, there].wait_recv()

    both = (0, 1)
    for half in both:
        spread(half, 0, 0, NEAR_FIRST)
    for half in both:
        spread(half, 1, 0)
    for half in both:
        across(half, 0, 0)
    for there in NEAR_FIRST:
        for half in both:
            arrive(half, 0, 0, there)
            spread(half, 1, there)
            across(half, there, 0)
    for there in NEAR_FIRST:
        for half in both:
            arrive(half, 1, 0, there)
            across(half, 0, there)

    def settle(chips):
        for half in both:
            for chip in chips:
                first, second = chip[::-1] if HALF_AXES[half][0] == "kv_1" else chip
                arrive(half, "across", first, second)

    settle(IN_LINE)
    if ready:
        ready(0)
    for first in NEAR_FIRST:
        for there in NEAR_FIRST:
            for half in both:
                arrive(half, 1, first, there)
                across(half, first, there)
    if ready:
        ready(1)
    settle(ASIDE)
    if ready:
        ready(2)


def axes_chip(half, first, second):
    return (second, first) if HALF_AXES[half][0] == "kv_1" else (first, second)


def add_up(wire, halves, value, last_out, last_in):
    copies = {}
    sums = [None, None]
    for turn, second in enumerate(FAR_FIRST):
        for half in (0, 1):
            count = halves[half][1]
            result = value(turn, half)
            if second == 0:
                sums[half] = result
                continue
            last_out[half, turn, pl.ds(0, count), :] = result.astype(BF16)
            copies[half, turn] = wire.send(
                last_out.at[half, turn, pl.ds(0, count), :],
                last_in.at[half, turn, pl.ds(0, count), :],
                HALF_AXES[half][1],
                second,
            )
    for turn in (1, 2, 0):
        for half in (0, 1):
            copies[half, turn].wait_recv()
            sums[half] += last_in[half, turn, pl.ds(0, halves[half][1]), :].astype(F32)
    return sums


def scatter_direct(wire, rows, term, between, buffers):
    halves = halves_of(rows)
    early_out, early_in, last_out, last_in = buffers
    copies = {}
    for turn, second in enumerate(FAR_FIRST):
        for way, step in enumerate(STEPS):
            for half in (0, 1):
                start, count, _ = halves[half]
                early_out[half, turn, way, pl.ds(0, count), :] = term(
                    axes_chip(half, step, second), start, count
                ).astype(BF16)
                copies[half, turn, way] = wire.send(
                    early_out.at[half, turn, way, pl.ds(0, count), :],
                    early_in.at[half, turn, way, pl.ds(0, count), :],
                    HALF_AXES[half][0],
                    step,
                )
        between(turn)

    def value(turn, half):
        start, count, _ = halves[half]
        result = term(axes_chip(half, 0, FAR_FIRST[turn]), start, count)
        for way in range(len(STEPS)):
            copies[half, turn, way].wait_recv()
            result += early_in[half, turn, way, pl.ds(0, count), :].astype(F32)
        return result

    return add_up(wire, halves, value, last_out, last_in)


def scatter_relayed(wire, rows, term, before, buffers):
    halves = halves_of(rows)
    early_out, early_in, late_out, late_in, last_out, last_in = buffers
    copies = {}

    def parts(half):
        _, count, cut = halves[half]
        return ((0, cut, 1), (cut, count - cut, 3))

    for half in (0, 1):
        before(half)
        for turn, second in enumerate(FAR_FIRST):
            start, count, _ = halves[half]
            early_out[half, turn, pl.ds(0, count), :] = term(
                axes_chip(half, 2, second), start, count
            ).astype(BF16)
            for at, length, step in parts(half):
                copies["early", half, turn, step] = wire.send(
                    early_out.at[half, turn, pl.ds(at, length), :],
                    early_in.at[half, turn, pl.ds(at, length), :],
                    HALF_AXES[half][0],
                    step,
                )
    for turn, second in enumerate(FAR_FIRST):
        for half in (0, 1):
            start, count, _ = halves[half]
            for way, (at, length, step) in enumerate(parts(half)):
                near = axes_chip(half, step, second)
                rest_at, rest = (length, count - length) if at == 0 else (0, at)
                late_out[half, turn, way, pl.ds(rest_at, rest), :] = term(
                    near, start + rest_at, rest
                ).astype(BF16)
                copies["early", half, turn, step].wait_recv()
                late_out[half, turn, way, pl.ds(at, length), :] = (
                    term(near, start + at, length)
                    + early_in[half, turn, pl.ds(at, length), :].astype(F32)
                ).astype(BF16)
                copies["late", half, turn, way] = wire.send(
                    late_out.at[half, turn, way, pl.ds(0, count), :],
                    late_in.at[half, turn, way, pl.ds(0, count), :],
                    HALF_AXES[half][0],
                    step,
                )

    def value(turn, half):
        start, count, _ = halves[half]
        result = term(axes_chip(half, 0, FAR_FIRST[turn]), start, count)
        for way in (0, 1):
            copies["late", half, turn, way].wait_recv()
            result += late_in[half, turn, way, pl.ds(0, count), :].astype(F32)
        return result

    return add_up(wire, halves, value, last_out, last_in)


def scatter_buffers(rows, relayed):
    half = halves_of(rows)[0][1]
    first = [(2, RING), (2, RING, 2)] if relayed else [(2, RING, len(STEPS))]
    return [
        pltpu.VMEM((*lead, half, LANES), BF16)
        for lead in (*first, (2, RING))
        for _ in (0, 1)
    ]


def load_feed_forward(place, gate_hbm, up_hbm, down_hbm, wide, down, sems):
    hidden = gate_hbm.shape[0]
    half = wide.shape[0] // 2
    for at, block in enumerate(ORDER):
        columns = pl.ds(pl.multiple_of(block_of(place, *block) * LANES, LANES), LANES)
        here = pl.ds(at * LANES, LANES)
        pltpu.make_async_copy(
            gate_hbm.at[:, columns], wide.at[pl.ds(0, hidden), here], sems.at[0]
        ).start()
        pltpu.make_async_copy(
            up_hbm.at[:, columns], wide.at[pl.ds(half, hidden), here], sems.at[1]
        ).start()
    for at, (along_0, along_1) in enumerate(CHIP_ORDER):
        for other in (0, 1):
            columns = pl.ds(
                pl.multiple_of(block_of(place, along_0, along_1, other) * LANES, LANES), LANES
            )
            pltpu.make_async_copy(
                down_hbm.at[:, columns],
                down.at[at // 2, :, pl.ds((at % 2 * 2 + other) * LANES, LANES)],
                sems.at[2],
            ).start()


def feed_forward(
    place, wire, held, gain, gate_hbm, up_hbm, down_hbm, wide, down, sems, scratch, buffers
):
    scaled, squares, gains, acc, own, pair_out, pair_in = scratch
    hidden, half = (gate_hbm.shape[0], wide.shape[0] // 2)
    rows, width = scaled.shape
    squares[...] = jnp.zeros_like(squares)
    for at, block in enumerate(ORDER):
        gains[pl.ds(at, 1), :] = gain[pl.ds(block_of(place, *block), 1), :]

    def scale(block, carry):
        entry = held[block].astype(F32)
        squares[...] += entry * entry
        scaled[:, pl.ds(pl.multiple_of(block * LANES, LANES), LANES)] = (
            entry * gains[pl.ds(block, 1), :]
        ).astype(BF16)
        return carry

    def ready(group):
        with jax.named_scope("scale_and_product"):
            first = sum(len(blocks) for blocks in GROUPS[:group])
            last = first + len(GROUPS[group])
            lax.fori_loop(first, last, scale, 0)
            if group == 0:
                pltpu.make_async_copy(gate_hbm, wide.at[pl.ds(0, hidden), :], sems.at[0]).wait()
                pltpu.make_async_copy(up_hbm, wide.at[pl.ds(half, hidden), :], sems.at[1]).wait()
            chunk = pl.ds(first * LANES, (last - first) * LANES)
            part = lax.dot_general(
                scaled[:, chunk],
                wide[:, chunk],
                (((1,), (1,)), ((), ())),
                preferred_element_type=F32,
            )
            acc[...] = part if group == 0 else acc[...] + part

    with jax.named_scope("gather_features"):
        gather(wire, held, ready)
    with jax.named_scope("hidden"):
        row_scale = lax.rsqrt(jnp.sum(squares[...], axis=1, keepdims=True) / width + epsilon)
        gate = row_scale * acc[:, :hidden]
        up = row_scale * acc[:, half : half + hidden]
        units = (gate / (1.0 + jnp.exp(-gate)) * up).astype(BF16)
        pltpu.make_async_copy(down, down, sems.at[2]).wait()
    pairs = CHIPS // 2
    first = wire.take(pairs)

    def pair_copy(at):
        part = pl.ds(2 * at, 2)
        return wire.make(pair_out.at[part], pair_in.at[part], "tp", 1, first + at)

    done = [0]

    def project(until):
        with jax.named_scope("down"):
            for at in range(done[0], until):
                result = jnp.dot(units, down[at], preferred_element_type=F32)
                for which in (0, 1):
                    at_lane = 2 * which * LANES
                    own[2 * at + which] = result[:, at_lane : at_lane + LANES]
                    pair_out[2 * at + which] = result[
                        :, at_lane + LANES : at_lane + 2 * LANES
                    ].astype(BF16)
                pair_copy(at).start()
            done[0] = max(done[0], until)

    arrived = set()

    def term(chip, start, count):
        at = POSITION[chip]
        if at // 2 not in arrived:
            arrived.add(at // 2)
            pair_copy(at // 2).wait_recv()
        return own[at, pl.ds(start, count), :] + pair_in[at, pl.ds(start, count), :].astype(F32)

    project(4)
    with jax.named_scope("scatter_features"):
        sums = scatter_direct(
            wire, rows, term, lambda turn: project((5, 8, 8, 8)[turn]), buffers
        )
    wire.sent += [pair_copy(at) for at in range(pairs)]
    return sums


def feed_forward_scratch(rows, width, hidden):
    half = -(-hidden // LANES) * LANES
    return [
        pltpu.VMEM((BLOCKS, rows, LANES), BF16),
        pltpu.VMEM((2 * half, width), BF16),
        pltpu.VMEM((CHIPS // 2, hidden, 4 * LANES), BF16),
        pltpu.SemaphoreType.DMA((10,)),
        pltpu.VMEM((rows, width), BF16),
        pltpu.VMEM((rows, LANES), F32),
        pltpu.VMEM((BLOCKS, LANES), F32),
        pltpu.VMEM((rows, 2 * half), F32),
        pltpu.VMEM((CHIPS, rows, LANES), F32),
        pltpu.VMEM((CHIPS, rows, LANES), BF16),
        pltpu.VMEM((CHIPS, rows, LANES), BF16),
        *scatter_buffers(rows, False),
    ]


def clear_padding(wide, hidden):
    half = wide.shape[0] // 2
    for start in (hidden, half + hidden):
        wide[pl.ds(start, half - hidden), :] = jnp.zeros((half - hidden, wide.shape[1]), BF16)


def first_kernel(
    tokens,
    gate_hbm,
    up_hbm,
    down_hbm,
    first_gain_hbm,
    mix_gain_hbm,
    query_hbm,
    forget_hbm,
    input_hbm,
    outgate_hbm,
    projected,
    mixer_share,
    send_sems,
    recv_sems,
    held,
    wide,
    down,
    sems,
    scaled,
    squares,
    gains,
    acc,
    own,
    pair_out,
    pair_in,
    *rest,
):
    buffers, own_refs, wide_buffers = (rest[:4], rest[4:13], rest[13:])
    low, high, share, ordered, wide_own, wide_out, wide_in, first_gain, mix_gain = own_refs
    place = own_place()
    wire = Wire(place, send_sems, recv_sems)
    own_tokens = pltpu.make_async_copy(tokens, held.at[0], sems.at[3])
    own_tokens.start()
    gain_loads = [
        pltpu.make_async_copy(first_gain_hbm, first_gain, sems.at[8]),
        pltpu.make_async_copy(mix_gain_hbm, mix_gain, sems.at[9]),
    ]
    for load in gain_loads:
        load.start()
    with jax.named_scope("greet"):
        wire.greet()
    own_tokens.wait()
    with jax.named_scope("issue_loads"):
        load_feed_forward(place, gate_hbm, up_hbm, down_hbm, wide, down, sems)
    width = query_hbm.shape[1]
    loads = [
        pltpu.make_async_copy(source, target.at[:, pl.ds(at, width)], sems.at[4 + index])
        for index, (source, target, at) in enumerate(
            (
                (query_hbm, low, 0),
                (forget_hbm, low, width),
                (input_hbm, high, 0),
                (outgate_hbm, high, width),
            )
        )
    ]
    for load in loads:
        load.start()
    clear_padding(wide, gate_hbm.shape[0])
    for load in gain_loads:
        load.wait()
    sums = feed_forward(
        place,
        wire,
        held,
        first_gain,
        gate_hbm,
        up_hbm,
        down_hbm,
        wide,
        down,
        sems,
        (scaled, squares, gains, acc, own, pair_out, pair_in),
        buffers,
    )
    rows = share.shape[0]
    for (start, count, _), value in zip(halves_of(rows), sums):
        part = pl.ds(start, count)
        mixed = (held[0, part, :].astype(F32) + 0.5 * value).astype(BF16)
        mixer_share[part, :] = mixed
        share[part, :] = mixed.astype(F32)
    seqs = rows // BLOCKS
    for block in range(BLOCKS):
        index = block_of(place, block // (2 * RING), block // 2 % RING, block % 2)
        ordered[pl.ds(block * seqs, seqs), :] = share[
            pl.ds(pl.multiple_of(index * seqs, seqs), seqs), :
        ]
    entry = ordered[...]
    index = block_of(place, 0, 0, 0)
    mix_scaled = (entry * mix_gain[pl.ds(index, 1), :]).astype(BF16)
    square_sum = jnp.broadcast_to(jnp.sum(entry * entry, axis=1, keepdims=True), entry.shape)
    for load in loads:
        load.wait()

    def keep(at, lower, upper):
        pair = jnp.concatenate(
            [lower.reshape(BLOCKS, seqs, LANES), upper.reshape(BLOCKS, seqs, LANES)], axis=1
        ).reshape(CHIPS, 2, 2 * seqs, LANES)
        wide_own[:, pl.ds(at, 2 * seqs), :] = pair[:, 0]
        wide_out[:, pl.ds(at, 2 * seqs), :] = pair[:, 1].astype(BF16)

    tile = 2 * seqs
    heads2 = low.shape[1] // LANES
    groups = (0, 5, 9, 13, heads2 // 2)
    copies = {}

    def project(group):
        with jax.named_scope("project"):
            for step in range(groups[group], groups[group + 1]):
                chunk = slice(2 * step * LANES, 2 * (step + 1) * LANES)
                lower = jnp.dot(mix_scaled, low[:, chunk], preferred_element_type=F32)
                upper = jnp.dot(mix_scaled, high[:, chunk], preferred_element_type=F32)
                for which in (0, 1):
                    lanes = slice(which * LANES, (which + 1) * LANES)
                    keep((2 * step + which) * tile, lower[:, lanes], upper[:, lanes])
            begin = 2 * groups[group] * tile
            end = 2 * groups[group + 1] * tile
            if group + 2 == len(groups):
                keep(end, square_sum, jnp.zeros_like(square_sum))
                end += tile
            part = pl.ds(begin, end - begin)
            copies[group] = wire.send(wide_out.at[:, part, :], wide_in.at[:, part, :], "tp", 1)

    def before(half):
        if half == 0:
            for group in (0, 1, 2):
                project(group)
        else:
            project(3)
        with jax.named_scope("pair"):
            for group in (2 * half, 2 * half + 1):
                copies[group].wait_recv()

    wide_rows = wide_own.shape[1]

    def term(chip, start, count):
        at = chip[0] * RING + chip[1]
        part = pl.ds(start, count)
        return wide_own[at, part, :] + wide_in[at, part, :].astype(F32)

    with jax.named_scope("scatter_wide"):
        sums = scatter_relayed(wire, wide_rows, term, before, wide_buffers)
    for (start, count, _), value in zip(halves_of(wide_rows), sums):
        projected[pl.ds(start, count), :] = value
    with jax.named_scope("finish"):
        wire.finish()


def state_kernel(
    full_width, projected, floor_grid, head_gain, state, next_state, mixer_out, held, sems
):
    seqs, heads, keys, values = state.shape
    tile = 2 * seqs
    writes = [
        pltpu.make_async_copy(held.at[head], next_state.at[:, head], sems.at[head])
        for head in range(heads)
    ]
    squares = projected[pl.ds(2 * heads * tile, seqs), :]
    scale = lax.rsqrt(squares / full_width + epsilon)

    def channels(block, second):
        return scale * projected[pl.ds(block * tile + second * seqs, seqs), :]

    row_seq = lax.broadcasted_iota(jnp.int32, (4 * seqs, seqs * values), 0) % seqs
    lane_seq = lax.broadcasted_iota(jnp.int32, (4 * seqs, seqs * values), 1) // values
    spreader = (row_seq == lane_seq).astype(F32).astype(BF16)

    def pieces(entry):
        first = entry.astype(BF16).astype(F32)
        second = (entry - first).astype(BF16).astype(F32)
        third = entry - first - second
        return jnp.concatenate([first, second, third, jnp.zeros_like(entry)], axis=0)

    for head in range(heads):
        query = channels(head, 0)
        entering = channels(head, 1)
        forget_pre = channels(heads + head, 0)
        gate = channels(heads + head, 1)
        floor = floor_grid[pl.ds(head, 1), :]
        forget = floor + (1.0 - floor) / (1.0 + jnp.exp(-forget_pre))
        query = query / (1.0 + jnp.exp(-query))
        both = jnp.concatenate([pieces(forget), pieces(query)], axis=1).T.astype(BF16)
        spread = jnp.dot(both, spreader, preferred_element_type=F32)
        readouts = []
        for seq in range(seqs):
            kept = spread[:keys, seq * values : (seq + 1) * values]
            asked = spread[keys:, seq * values : (seq + 1) * values]
            after = kept * state[seq, head] + (1.0 - kept) * entering[seq : seq + 1, :]
            held[head, seq] = after
            readouts.append(jnp.sum(after * asked, axis=0, keepdims=True))
        writes[head].start()
        readout = jnp.concatenate(readouts, axis=0)
        normed = (
            readout
            * lax.rsqrt(jnp.mean(readout * readout, axis=-1, keepdims=True) + epsilon)
            * head_gain[...]
        )
        half = heads // 2
        row = head % half * tile + head // half * seqs
        mixer_out[pl.ds(row, seqs), :] = normed * (gate / (1.0 + jnp.exp(-gate)))
    for write in writes:
        write.wait()


def second_kernel(
    mixer_out,
    share_hbm,
    output_hbm,
    gate_hbm,
    up_hbm,
    down_hbm,
    gain_hbm,
    layer_out,
    send_sems,
    recv_sems,
    held,
    wide,
    down,
    sems,
    scaled,
    squares,
    gains,
    acc,
    own,
    pair_out,
    pair_in,
    *rest,
):
    buffers, (mixed, output, update, mixer_share, second_gain) = rest[:4], rest[4:]
    place = own_place()
    wire = Wire(place, send_sems, recv_sems)
    depth = output.shape[0]
    loads = [
        pltpu.make_async_copy(
            output_hbm.at[pl.ds(which * depth, depth), :],
            output.at[:, pl.ds(which * LANES, LANES)],
            sems.at[3 + which],
        )
        for which in (0, 1)
    ] + [
        pltpu.make_async_copy(share_hbm, mixer_share, sems.at[5]),
        pltpu.make_async_copy(gain_hbm, second_gain, sems.at[6]),
    ]
    for load in loads:
        load.start()
    mixed[0] = mixer_out[...].astype(BF16)
    with jax.named_scope("greet"):
        wire.greet()
    with jax.named_scope("issue_loads"):
        load_feed_forward(place, gate_hbm, up_hbm, down_hbm, wide, down, sems)
    clear_padding(wide, gate_hbm.shape[0])
    with jax.named_scope("gather_mixed"):
        gather(wire, mixed)
    for load in loads:
        load.wait()
    rows = update.shape[0]
    seqs = rows // BLOCKS
    tile = 2 * seqs
    total = None
    for step in range(depth // (2 * LANES)):
        pieces = [
            mixed[:, pl.ds((2 * step + which) * tile, tile), :].reshape(
                BLOCKS * tile, LANES
            )
            for which in (0, 1)
        ]
        product = jnp.dot(
            jnp.concatenate(pieces, axis=1),
            output[pl.ds(step * 2 * LANES, 2 * LANES), :],
            preferred_element_type=F32,
        )
        total = product if total is None else total + product
    total = total.reshape(BLOCKS, tile, 2 * LANES)
    total = total[:, :seqs, :LANES] + total[:, seqs:, LANES:]
    for block in range(BLOCKS):
        index = block_of(place, *ORDER[block])
        update[pl.ds(pl.multiple_of(index * seqs, seqs), seqs), :] = total[block]
    held[0] = (mixer_share[...].astype(F32) + update[...]).astype(BF16)
    sums = feed_forward(
        place,
        wire,
        held,
        second_gain,
        gate_hbm,
        up_hbm,
        down_hbm,
        wide,
        down,
        sems,
        (scaled, squares, gains, acc, own, pair_out, pair_in),
        buffers,
    )
    for (start, count, _), value in zip(halves_of(rows), sums):
        part = pl.ds(start, count)
        layer_out[part, :] = (held[0, part, :].astype(F32) + 0.5 * value).astype(BF16)
    with jax.named_scope("finish"):
        wire.finish()


def in_space(*spaces):
    return [pl.BlockSpec(memory_space=space) for space in spaces]


def kernel_params(identity, mebibytes):
    return pltpu.CompilerParams(
        collective_id=identity, has_side_effects=True, vmem_limit_bytes=mebibytes << 20
    )


def per_device(
    tokens,
    carried_state,
    first_gain,
    first_gate,
    first_up,
    first_down,
    mix_gain,
    query_weight,
    forget_weight,
    input_weight,
    outgate_weight,
    forget_floor,
    head_gain,
    output_weight,
    second_gain,
    second_gate,
    second_up,
    second_down,
):
    rows, share = tokens.shape
    full_width, hidden = first_gate.shape
    seqs, heads, keys, values = carried_state.shape
    tile = 2 * seqs
    wide_rows = (2 * heads + 1) * tile
    by_block = (full_width // LANES, LANES)
    projected, mixer_share = pl.pallas_call(
        first_kernel,
        name="first_block",
        out_shape=(
            jax.ShapeDtypeStruct((wide_rows, LANES), F32),
            jax.ShapeDtypeStruct((rows, share), BF16),
        ),
        in_specs=in_space(*(HBM,) * 10),
        out_specs=in_space(VMEM, VMEM),
        scratch_shapes=[
            pltpu.SemaphoreType.DMA((192,)),
            pltpu.SemaphoreType.DMA((192,)),
            *feed_forward_scratch(rows, full_width, hidden),
            pltpu.VMEM((share, 2 * heads * keys), BF16),
            pltpu.VMEM((share, 2 * heads * values), BF16),
            pltpu.VMEM((rows, LANES), F32),
            pltpu.VMEM((rows, LANES), F32),
            pltpu.VMEM((CHIPS, wide_rows, LANES), F32),
            pltpu.VMEM((CHIPS, wide_rows, LANES), BF16),
            pltpu.VMEM((CHIPS, wide_rows, LANES), BF16),
            pltpu.VMEM(by_block, F32),
            pltpu.VMEM(by_block, F32),
            *scatter_buffers(wide_rows, True),
        ],
        compiler_params=kernel_params(0, 54),
    )(
        tokens,
        first_gate.T,
        first_up.T,
        first_down,
        first_gain.reshape(by_block),
        mix_gain.reshape(by_block),
        query_weight,
        forget_weight,
        input_weight,
        outgate_weight,
    )
    next_state, mixer_out = pl.pallas_call(
        lambda *refs: state_kernel(full_width, *refs),
        name="state_update",
        out_shape=(
            jax.ShapeDtypeStruct(carried_state.shape, F32),
            jax.ShapeDtypeStruct((heads * seqs, values), F32),
        ),
        in_specs=in_space(VMEM, VMEM, VMEM, VMEM),
        out_specs=in_space(HBM, VMEM),
        scratch_shapes=[
            pltpu.VMEM((heads, seqs, keys, values), F32),
            pltpu.SemaphoreType.DMA((heads,)),
        ],
        compiler_params=pltpu.CompilerParams(vmem_limit_bytes=12 << 20),
    )(
        projected,
        forget_floor.reshape(heads, keys),
        head_gain.reshape(1, values),
        carried_state,
    )
    layer_out = pl.pallas_call(
        second_kernel,
        name="second_block",
        out_shape=jax.ShapeDtypeStruct((rows, share), BF16),
        in_specs=in_space(VMEM, *(HBM,) * 6),
        out_specs=pl.BlockSpec(memory_space=VMEM),
        scratch_shapes=[
            pltpu.SemaphoreType.DMA((224,)),
            pltpu.SemaphoreType.DMA((224,)),
            *feed_forward_scratch(rows, full_width, hidden),
            pltpu.VMEM((BLOCKS, heads * seqs, LANES), BF16),
            pltpu.VMEM((heads * values // 2, 2 * LANES), BF16),
            pltpu.VMEM((rows, LANES), F32),
            pltpu.VMEM((rows, LANES), BF16),
            pltpu.VMEM(by_block, F32),
        ],
        compiler_params=kernel_params(1, 58),
    )(
        mixer_out,
        mixer_share,
        output_weight,
        second_gate.T,
        second_up.T,
        second_down,
        second_gain.reshape(by_block),
    )
    return (layer_out, next_state)


def solution(mesh):
    split = Mesh(
        mesh.devices.reshape(mesh.shape["dp"], RING, RING, mesh.shape["tp"]), DP_KV_TP
    )
    return jax.shard_map(
        per_device,
        mesh=split,
        in_specs=(
            P("dp", KV_TP),
            P(DP_KV_TP, None, None, None),
            P(),
            P(None, KV_TP),
            P(None, KV_TP),
            P(KV_TP, None),
            P(),
            P(KV_TP, None),
            P(KV_TP, None),
            P(KV_TP, None),
            P(KV_TP, None),
            P(),
            P(),
            P(None, KV_TP),
            P(),
            P(None, KV_TP),
            P(None, KV_TP),
            P(KV_TP, None),
        ),
        out_specs=(P("dp", KV_TP), P(DP_KV_TP, None, None, None)),
        check_vma=False,
    )
```

time: 147 us -> 104 us (0.71)
  Pallas kernels: 145 us -> 100 us
  local copies, waits for them, and re-layouts: 1.47 us -> 3.06 us
    pallas_call x1, Pallas kernels: 70.1 us -> 54 us  [per_device(): pl.pallas_call(first_kernel, name='first_block', out_shape=(jax.ShapeDtyp...]
    pallas_call x1, Pallas kernels: 57.7 us -> 42.3 us  [per_device(): pl.pallas_call(second_kernel, name='second_block', out_shape=jax.ShapeDty...]
    pallas_call x1, Pallas kernels: 16.9 us -> 3.78 us  [per_device(): pl.pallas_call(lambda *refs: state_kernel(full_width, *refs), name='state...]
    unnamed x1 -> x11, local copies, waits for them, and re-layouts: 1.47 us -> 3.06 us
where the time goes in v2:
time: 104 us
  Pallas kernels  100 us (96%)
  local copies, waits for them, and re-layouts  3.06 us (3%)
    pallas_call x1, Pallas kernels, per_device(): pl.pallas_call(first_kernel, name='first_block', out_shape=(jax.ShapeDtyp...  54 us
    pallas_call x1, Pallas kernels, per_device(): pl.pallas_call(second_kernel, name='second_block', out_shape=jax.ShapeDty...  42.3 us
    pallas_call x1, Pallas kernels, per_device(): pl.pallas_call(lambda *refs: state_kernel(full_width, *refs), name='state...  3.78 us
    unnamed x11, local copies, waits for them, and re-layouts  3.06 us

profile of v2, /device:TPU:0, one launch (start us, length us, event | category | flops | bytes accessed | tf_op | source)
XLA Modules:
  0.0 103.9 jit_solution(14015751442000139624)
XLA Ops:
  0.6 0.0 copy-start
  0.6 0.0 copy-start.3
  0.7 0.0 copy-start.4
  0.7 54.0 %first_block.1 = (f32[528,128]{1,0:T(8,128)}, bf16[256,128]{1,0:T(8,128)(2,1)}) custom-call(bf16[256,128]{1,0:T(8,128)(2,1)} %tokens.1, bf16[352,4096]{1,0:T(8,128)(2,1)} %bitcast.11, bf16[352,4096]{1,0:T(8,128)(2,1)} %bitcast.12, bf16[352,4096]{1,0:T(8,128)(2,1)} %down_hbm.2, f32[32,128]{1,0:T(8,128)} %bitcast.15, f32[32,128]{1,0:T(8,128)} %bitcast.16, ...), custom_call_target="tpu_custom_call" | custom-call | tf_op jit(solution)/shard_map/first_block/pallas_call | solution.py:766
  54.7 0.0 copy-done
  54.7 0.0 copy-done.3
  54.7 0.0 copy-done.4
  54.7 0.0 copy-start.1
  54.7 0.9 copy-done.1
  55.6 3.8 %state_update.1 = (f32[8,16,128,128]{3,2,1,0:T(8,128)}, f32[128,128]{1,0:T(8,128)S(1)}) custom-call(f32[528,128]{1,0:T(8,128)S(1)} %copy-done.1, f32[16,128]{1,0:T(8,128)S(1)} %bitcast.9, f32[1,128]{1,0:T(1,128)S(1)} %bitcast.10, f32[8,16,128,128]{3,2,1,0:T(8,128)S(1)} %copy-done), custom_call_target="tpu_custom_call" | custom-call | tf_op jit(solution)/shard_map/state_update/pallas_call | solution.py:803
  59.4 0.0 copy-start.2
  59.5 0.6 copy-done.2
  60.1 42.3 %second_block.1 = bf16[256,128]{1,0:T(8,128)(2,1)} custom-call(f32[128,128]{1,0:T(8,128)} %copy-done.2, bf16[256,128]{1,0:T(8,128)(2,1)} %get-tuple-element.8.share_hbm, bf16[2048,128]{1,0:T(8,128)(2,1)} %output_hbm.1, bf16[352,4096]{1,0:T(8,128)(2,1)} %bitcast.13, bf16[352,4096]{1,0:T(8,128)(2,1)} %bitcast.14, bf16[352,4096]{1,0:T(8,128)(2,1)} %down_hbm.3, ...), custom_call_target="tpu_custom_call" | custom-call | tf_op jit(solution)/shard_map/second_block/pallas_call | solution.py:823
  102.4 1.5 %copy.21 = bf16[256,128]{1,0:T(8,128)(2,1)} copy(bf16[256,128]{1,0:T(8,128)(2,1)} %second_block.1) | data formatting | bytes 131072
Async XLA Ops:
  0.6 54.0 %copy-start = (f32[8,16,128,128]{3,2,1,0:T(8,128)S(1)}, f32[8,16,128,128]{3,2,1,0:T(8,128)}, u32[]{:S(2)}) copy-start(f32[8,16,128,128]{3,2,1,0:T(8,128)} %refs_3_.1) | copy-start | bytes 25165828
  0.6 54.0 %copy-start.3 = (f32[2048]{0:T(1024)S(1)}, f32[2048]{0:T(1024)}, u32[]{:S(2)}) copy-start(f32[2048]{0:T(1024)} %param.29) | copy-start | bytes 24580
  0.7 54.0 %copy-start.4 = (f32[128]{0:T(128)S(1)}, f32[128]{0:T(128)}, u32[]{:S(2)}) copy-start(f32[128]{0:T(128)} %param.30) | copy-start | bytes 1540
  54.7 1.0 copy-start.1
  59.4 0.6 copy-start.2

commit v3 on v2

--- a/solution.py
+++ b/solution.py
@@ -25,13 +25,13 @@
 NEAR_FIRST = (1, 3, 2)
 STEPS = (2, 1, 3)
 IN_LINE = ((0, 0),) + tuple((0, a) for a in NEAR_FIRST) + tuple((a, 0) for a in NEAR_FIRST)
-ASIDE = tuple((a, b) for a in NEAR_FIRST for b in NEAR_FIRST)
+EARLY = tuple((a, b) for a in (1, 3) for b in (1, 3))
+LATE = tuple((a, 2) for a in (1, 3)) + tuple((2, a) for a in NEAR_FIRST)
 GROUPS = (
     tuple((*chip, core) for core in (0, 1) for chip in IN_LINE),
-    tuple((*chip, 0) for chip in ASIDE),
-    tuple((*chip, 1) for chip in ASIDE),
+    *(tuple((*chip, core) for chip in chips) for chips in (EARLY, LATE) for core in (0, 1)),
 )
-ORDER = GROUPS[0] + GROUPS[1] + GROUPS[2]
+ORDER = sum(GROUPS, ())
 KEPT_AT = {block: at for at, block in enumerate(ORDER)}
 FIRST_CHIPS = tuple(
     chip
@@ -68,12 +68,13 @@
         at, size = self.place[axis]
         return {axis: lax.rem(at + step, size)}
 
-    def greet(self):
+    def greet(self, meanwhile):
         barrier = pltpu.get_barrier_semaphore()
         for axis, step in NEAR:
             pl.semaphore_signal(
                 barrier, inc=1, device_id=self.near(axis, step), device_id_type=MESH
             )
+        meanwhile()
         pl.semaphore_wait(barrier, len(NEAR))
 
     def take(self, count):
@@ -158,19 +159,25 @@
                 first, second = chip[::-1] if HALF_AXES[half][0] == "kv_1" else chip
                 arrive(half, "across", first, second)
 
+    def pass_on(firsts, theres):
+        for first in firsts:
+            for there in theres:
+                for half in both:
+                    arrive(half, 1, first, there)
+                    across(half, first, there)
+
+    ready = ready or (lambda group: None)
     settle(IN_LINE)
-    if ready:
-        ready(0)
-    for first in NEAR_FIRST:
-        for there in NEAR_FIRST:
-            for half in both:
-                arrive(half, 1, first, there)
-                across(half, first, there)
-    if ready:
-        ready(1)
-    settle(ASIDE)
-    if ready:
-        ready(2)
+    ready(0)
+    pass_on((1, 3), (1, 3))
+    ready(1)
+    pass_on((1, 3), (2,))
+    pass_on((2,), (1, 3, 2))
+    settle(EARLY)
+    ready(2)
+    ready(3)
+    settle(LATE)
+    ready(4)
 
 
 def axes_chip(half, first, second):
@@ -231,7 +238,7 @@
     return add_up(wire, halves, value, last_out, last_in)
 
 
-def scatter_relayed(wire, rows, term, before, buffers):
+def scatter_relayed(wire, rows, term, buffers):
     halves = halves_of(rows)
     early_out, early_in, late_out, late_in, last_out, last_in = buffers
     copies = {}
@@ -241,7 +248,6 @@
         return ((0, cut, 1), (cut, count - cut, 3))
 
     for half in (0, 1):
-        before(half)
         for turn, second in enumerate(FAR_FIRST):
             start, count, _ = halves[half]
             early_out[half, turn, pl.ds(0, count), :] = term(
@@ -468,10 +474,10 @@
     for load in gain_loads:
         load.start()
     with jax.named_scope("greet"):
-        wire.greet()
+        wire.greet(
+            lambda: load_feed_forward(place, gate_hbm, up_hbm, down_hbm, wide, down, sems)
+        )
     own_tokens.wait()
-    with jax.named_scope("issue_loads"):
-        load_feed_forward(place, gate_hbm, up_hbm, down_hbm, wide, down, sems)
     width = query_hbm.shape[1]
     loads = [
         pltpu.make_async_copy(source, target.at[:, pl.ds(at, width)], sems.at[4 + index])
@@ -525,51 +531,58 @@
     def keep(at, lower, upper):
         pair = jnp.concatenate(
             [lower.reshape(BLOCKS, seqs, LANES), upper.reshape(BLOCKS, seqs, LANES)], axis=1
-        ).reshape(CHIPS, 2, 2 * seqs, LANES)
-        wide_own[:, pl.ds(at, 2 * seqs), :] = pair[:, 0]
-        wide_out[:, pl.ds(at, 2 * seqs), :] = pair[:, 1].astype(BF16)
+        ).reshape(RING, RING, 2, 2 * seqs, LANES)
+        wide_own[:, :, pl.ds(at, 2 * seqs), :] = pair[:, :, 0]
+        wide_out[:, :, pl.ds(at, 2 * seqs), :] = pair[:, :, 1].astype(BF16)
 
     tile = 2 * seqs
-    heads2 = low.shape[1] // LANES
-    groups = (0, 5, 9, 13, heads2 // 2)
+    wide_rows = wide_own.shape[2]
+    wide_halves = halves_of(wide_rows)
+    columns = low.shape[1] // LANES
     copies = {}
 
-    def project(group):
+    def project(steps):
         with jax.named_scope("project"):
-            for step in range(groups[group], groups[group + 1]):
+            for step in steps:
                 chunk = slice(2 * step * LANES, 2 * (step + 1) * LANES)
                 lower = jnp.dot(mix_scaled, low[:, chunk], preferred_element_type=F32)
                 upper = jnp.dot(mix_scaled, high[:, chunk], preferred_element_type=F32)
                 for which in (0, 1):
                     lanes = slice(which * LANES, (which + 1) * LANES)
                     keep((2 * step + which) * tile, lower[:, lanes], upper[:, lanes])
-            begin = 2 * groups[group] * tile
-            end = 2 * groups[group + 1] * tile
-            if group + 2 == len(groups):
-                keep(end, square_sum, jnp.zeros_like(square_sum))
-                end += tile
-            part = pl.ds(begin, end - begin)
-            copies[group] = wire.send(wide_out.at[:, part, :], wide_in.at[:, part, :], "tp", 1)
-
-    def before(half):
-        if half == 0:
-            for group in (0, 1, 2):
-                project(group)
-        else:
-            project(3)
-        with jax.named_scope("pair"):
-            for group in (2 * half, 2 * half + 1):
-                copies[group].wait_recv()
-
-    wide_rows = wide_own.shape[1]
+
+    def across(half, first):
+        part = pl.ds(*wide_halves[half][:2])
+        chips = (slice(None), first) if HALF_AXES[half][0] == "kv_1" else (first, slice(None))
+        copies[half, first] = wire.send(
+            wide_out.at[(*chips, part, slice(None))],
+            wide_in.at[(*chips, part, slice(None))],
+            "tp",
+            1,
+        )
+
+    first_steps = -(-wide_halves[0][1] // (2 * tile))
+    project(range(first_steps))
+    across(0, 2)
+    project(range(first_steps, columns // 2))
+    keep(columns * tile, square_sum, jnp.zeros_like(square_sum))
+    across(1, 2)
+    for first in (1, 3, 0):
+        for half in (0, 1):
+            across(half, first)
+    arrived = set()
 
     def term(chip, start, count):
-        at = chip[0] * RING + chip[1]
+        half = 0 if start < wide_halves[1][0] else 1
+        first = chip[1] if HALF_AXES[half][0] == "kv_1" else chip[0]
+        if (half, first) not in arrived:
+            arrived.add((half, first))
+            copies[half, first].wait_recv()
         part = pl.ds(start, count)
-        return wide_own[at, part, :] + wide_in[at, part, :].astype(F32)
+        return wide_own[(*chip, part)] + wide_in[(*chip, part)].astype(F32)
 
     with jax.named_scope("scatter_wide"):
-        sums = scatter_relayed(wire, wide_rows, term, before, wide_buffers)
+        sums = scatter_relayed(wire, wide_rows, term, wide_buffers)
     for (start, count, _), value in zip(halves_of(wide_rows), sums):
         projected[pl.ds(start, count), :] = value
     with jax.named_scope("finish"):
@@ -675,9 +688,9 @@
         load.start()
     mixed[0] = mixer_out[...].astype(BF16)
     with jax.named_scope("greet"):
-        wire.greet()
-    with jax.named_scope("issue_loads"):
-        load_feed_forward(place, gate_hbm, up_hbm, down_hbm, wide, down, sems)
+        wire.greet(
+            lambda: load_feed_forward(place, gate_hbm, up_hbm, down_hbm, wide, down, sems)
+        )
     clear_padding(wide, gate_hbm.shape[0])
     with jax.named_scope("gather_mixed"):
         gather(wire, mixed)
@@ -759,6 +772,7 @@
 ):
     rows, share = tokens.shape
     full_width, hidden = first_gate.shape
+    in_hbm = lambda array: pltpu.with_memory_space_constraint(array, HBM)
     seqs, heads, keys, values = carried_state.shape
     tile = 2 * seqs
     wide_rows = (2 * heads + 1) * tile
@@ -780,25 +794,25 @@
             pltpu.VMEM((share, 2 * heads * values), BF16),
             pltpu.VMEM((rows, LANES), F32),
             pltpu.VMEM((rows, LANES), F32),
-            pltpu.VMEM((CHIPS, wide_rows, LANES), F32),
-            pltpu.VMEM((CHIPS, wide_rows, LANES), BF16),
-            pltpu.VMEM((CHIPS, wide_rows, LANES), BF16),
+            pltpu.VMEM((RING, RING, wide_rows, LANES), F32),
+            pltpu.VMEM((RING, RING, wide_rows, LANES), BF16),
+            pltpu.VMEM((RING, RING, wide_rows, LANES), BF16),
             pltpu.VMEM(by_block, F32),
             pltpu.VMEM(by_block, F32),
             *scatter_buffers(wide_rows, True),
         ],
-        compiler_params=kernel_params(0, 54),
+        compiler_params=kernel_params(0, 44),
     )(
-        tokens,
-        first_gate.T,
-        first_up.T,
-        first_down,
-        first_gain.reshape(by_block),
-        mix_gain.reshape(by_block),
-        query_weight,
-        forget_weight,
-        input_weight,
-        outgate_weight,
+        in_hbm(tokens),
+        in_hbm(first_gate.T),
+        in_hbm(first_up.T),
+        in_hbm(first_down),
+        in_hbm(first_gain.reshape(by_block)),
+        in_hbm(mix_gain.reshape(by_block)),
+        in_hbm(query_weight),
+        in_hbm(forget_weight),
+        in_hbm(input_weight),
+        in_hbm(outgate_weight),
     )
     next_state, mixer_out = pl.pallas_call(
         lambda *refs: state_kernel(full_width, *refs),
@@ -836,15 +850,15 @@
             pltpu.VMEM((rows, LANES), BF16),
             pltpu.VMEM(by_block, F32),
         ],
-        compiler_params=kernel_params(1, 58),
+        compiler_params=kernel_params(1, 32),
     )(
         mixer_out,
         mixer_share,
-        output_weight,
-        second_gate.T,
-        second_up.T,
-        second_down,
-        second_gain.reshape(by_block),
+        in_hbm(output_weight),
+        in_hbm(second_gate.T),
+        in_hbm(second_up.T),
+        in_hbm(second_down),
+        in_hbm(second_gain.reshape(by_block)),
     )
     return (layer_out, next_state)
 

time: 104 us -> 96.7 us (0.930)
  Pallas kernels: 100 us -> 94.4 us
  local copies, waits for them, and re-layouts: 3.06 us -> 0.64 us
    pallas_call x1, Pallas kernels: 42.3 us -> 39.1 us  [per_device(): pl.pallas_call(second_kernel, name='second_block', out_shape=jax.ShapeDty...]
    pallas_call x1, Pallas kernels: 54 us -> 51.5 us  [per_device(): pl.pallas_call(first_kernel, name='first_block', out_shape=(jax.ShapeDtyp...]
    unnamed x11 -> x7, local copies, waits for them, and re-layouts: 3.06 us -> 0.64 us
where the time goes in v3:
time: 96.7 us; the launch traced here: 95.8 us
  Pallas kernels  94.4 us (98%)
    pallas_call x1, Pallas kernels, per_device(): pl.pallas_call(first_kernel, name='first_block', out_shape=(jax.ShapeDtyp...  51.5 us
    pallas_call x1, Pallas kernels, per_device(): pl.pallas_call(second_kernel, name='second_block', out_shape=jax.ShapeDty...  39.1 us
    pallas_call x1, Pallas kernels, per_device(): pl.pallas_call(lambda *refs: state_kernel(full_width, *refs), name='state...  3.79 us

profile of v3, /device:TPU:0, one launch (start us, length us, event | category | flops | bytes accessed | tf_op | source)
XLA Modules:
  0.0 95.8 jit_solution(3281458459083428414)
XLA Ops:
  0.6 0.0 copy-start
  0.6 0.0 copy-start.1
  0.7 0.0 copy-start.2
  0.7 51.5 %first_block.1 = (f32[528,128]{1,0:T(8,128)S(1)}, bf16[256,128]{1,0:T(8,128)(2,1)S(1)}) custom-call(bf16[256,128]{1,0:T(8,128)(2,1)} %tokens.1, bf16[352,4096]{1,0:T(8,128)(2,1)} %bitcast.11, bf16[352,4096]{1,0:T(8,128)(2,1)} %bitcast.12, bf16[352,4096]{1,0:T(8,128)(2,1)} %down_hbm.2, f32[32,128]{1,0:T(8,128)} %bitcast.15, f32[32,128]{1,0:T(8,128)} %bitcast.16, ...), custom_call_target="tpu_custom_call" | custom-call | tf_op jit(solution)/shard_map/first_block/pallas_call | solution.py:780
  52.2 0.0 copy-done
  52.2 0.0 copy-done.1
  52.2 0.0 copy-done.2
  52.2 3.8 %state_update.1 = (f32[8,16,128,128]{3,2,1,0:T(8,128)}, f32[128,128]{1,0:T(8,128)S(1)}) custom-call(f32[528,128]{1,0:T(8,128)S(1)} %get-tuple-element.6.refs_0_, f32[16,128]{1,0:T(8,128)S(1)} %bitcast.9, f32[1,128]{1,0:T(1,128)S(1)} %bitcast.10, f32[8,16,128,128]{3,2,1,0:T(8,128)S(1)} %copy-done), custom_call_target="tpu_custom_call" | custom-call | tf_op jit(solution)/shard_map/state_update/pallas_call | solution.py:817
  56.0 39.1 %second_block.1 = bf16[256,128]{1,0:T(8,128)(2,1)S(1)} custom-call(f32[128,128]{1,0:T(8,128)S(1)} %get-tuple-element.7.mixer_out, bf16[256,128]{1,0:T(8,128)(2,1)S(1)} %get-tuple-element.8.share_hbm, bf16[2048,128]{1,0:T(8,128)(2,1)} %output_hbm.1, bf16[352,4096]{1,0:T(8,128)(2,1)} %bitcast.13, bf16[352,4096]{1,0:T(8,128)(2,1)} %bitcast.14, ...), custom_call_target="tpu_custom_call" | custom-call | tf_op jit(solution)/shard_map/second_block/pallas_call | solution.py:837
  95.2 0.6 copy.21
Async XLA Ops:
  0.6 51.5 %copy-start = (f32[8,16,128,128]{3,2,1,0:T(8,128)S(1)}, f32[8,16,128,128]{3,2,1,0:T(8,128)}, u32[]{:S(2)}) copy-start(f32[8,16,128,128]{3,2,1,0:T(8,128)} %refs_3_.1) | copy-start | bytes 25165828
  0.6 51.5 %copy-start.1 = (f32[2048]{0:T(1024)S(1)}, f32[2048]{0:T(1024)}, u32[]{:S(2)}) copy-start(f32[2048]{0:T(1024)} %param.29) | copy-start | bytes 24580
  0.7 51.5 %copy-start.2 = (f32[128]{0:T(128)S(1)}, f32[128]{0:T(128)}, u32[]{:S(2)}) copy-start(f32[128]{0:T(128)} %param.30) | copy-start | bytes 1540

commit v4 on v3

--- a/solution.py
+++ b/solution.py
@@ -18,8 +18,12 @@
 RING = 4
 LANES = 128
 CHIPS = RING * RING
+WIDE_PIECES = 4
 BLOCKS = 2 * CHIPS
-NEAR = tuple((axis, step) for axis in ("kv_0", "kv_1") for step in (2, 1, 3)) + (("tp", 1),)
+NEAR = (
+    *((axis, step, 0) for axis in ("kv_0", "kv_1") for step in (2, 1, 3)),
+    ("tp", 1, 0),
+)
 HALF_AXES = (("kv_1", "kv_0"), ("kv_0", "kv_1"))
 FAR_FIRST = (2, 1, 3, 0)
 NEAR_FIRST = (1, 3, 2)
@@ -43,6 +47,10 @@
 POSITION = {chip: place for place, chip in enumerate(CHIP_ORDER)}
 
 
+def crosses(chip):
+    return 0
+
+
 def own_place():
     return (lax.axis_index("kv_0"), lax.axis_index("kv_1"), lax.axis_index("tp"))
 
@@ -64,15 +72,18 @@
         self.used = 0
         self.sent = []
 
-    def near(self, axis, step):
+    def near(self, axis, step, cross):
         at, size = self.place[axis]
-        return {axis: lax.rem(at + step, size)}
+        there = {axis: lax.rem(at + step, size)}
+        if cross:
+            there["tp"] = 1 - self.place["tp"][0]
+        return there
 
     def greet(self, meanwhile):
         barrier = pltpu.get_barrier_semaphore()
-        for axis, step in NEAR:
+        for axis, step, cross in NEAR:
             pl.semaphore_signal(
-                barrier, inc=1, device_id=self.near(axis, step), device_id_type=MESH
+                barrier, inc=1, device_id=self.near(axis, step, cross), device_id_type=MESH
             )
         meanwhile()
         pl.semaphore_wait(barrier, len(NEAR))
@@ -82,55 +93,68 @@
         self.used += count
         return first
 
-    def make(self, source, target, axis, step, slot):
+    def make(self, source, target, axis, step, slot, cross=0):
         return pltpu.make_async_remote_copy(
             src_ref=source,
             dst_ref=target,
             send_sem=self.send_sems.at[slot],
             recv_sem=self.recv_sems.at[slot],
-            device_id=self.near(axis, step),
+            device_id=self.near(axis, step, cross),
             device_id_type=MESH,
         )
 
-    def send(self, source, target, axis, step):
-        copy = self.make(source, target, axis, step, self.take(1))
+    def send(self, source, target, axis, step, cross=None):
+        cross = 0
+        copy = self.make(source, target, axis, step, self.take(1), cross)
         copy.start()
         self.sent.append(copy)
         return copy
 
-    def finish(self):
-        for copy in self.sent:
+    def finish(self, count=None):
+        for copy in self.sent[:count]:
             copy.wait_send()
-        self.sent = []
-
-
-def halves_of(rows):
+        self.sent = self.sent[count:] if count is not None else []
+
+
+def pieces_of(rows, number=2):
     tiles = rows // 16
-    first = (tiles - tiles // 2) * 16
-    second = rows - first
-    return ((0, first, first // 32 * 16), (first, second, second // 32 * 16))
-
-
-def gather(wire, held, ready=None):
-    halves = halves_of(held.shape[1])
+    ends = [-(-tiles * piece // number) * 16 for piece in range(number + 1)]
+    return tuple((a, b - a, (b - a) // 32 * 16) for a, b in zip(ends, ends[1:]))
+
+
+def axes_of(piece):
+    return HALF_AXES[piece % 2]
+
+
+def axes_chip(half, first, second):
+    return (second, first) if axes_of(half)[0] == "kv_1" else (first, second)
+
+
+def gather(wire, held, ready, eager, started=lambda: None):
+    halves = pieces_of(held.shape[1])
     copies = {}
 
-    def view(half, first, second, core=0):
+    def view(half, first, second, core):
         start, rows, _ = halves[half]
-        along = (second, first) if HALF_AXES[half][0] == "kv_1" else (first, second)
-        return held.at[KEPT_AT[(*along, core)], pl.ds(start, rows), :]
+        chip = axes_chip(half, first, second)
+        return held.at[KEPT_AT[(*chip, core)], pl.ds(start, rows), :]
 
     def spread(half, stage, first, steps=STEPS):
         for step in steps:
             there = RING - step
-            target = view(half, there, 0) if stage == 0 else view(half, first, there)
+            chip = (there, 0) if stage == 0 else (first, there)
+            source = (0, 0) if stage == 0 else (first, 0)
             copies[half, stage, first, there] = wire.send(
-                view(half, first, 0), target, HALF_AXES[half][stage], step
+                view(half, *source, crosses(source)),
+                view(half, *chip, crosses(chip)),
+                axes_of(half)[stage],
+                step,
             )
 
     def across(half, first, second):
+        core = crosses((first, second))
         copies[half, "across", first, second] = wire.send(
-            view(half, first, second), view(half, first, second, 1), "tp", 1
+            view(half, first, second, core), view(half, first, second, 1 - core), "tp", 1
         )
 
     def arrive(half, stage, first, there):
@@ -143,6 +167,7 @@
         spread(half, 1, 0)
     for half in both:
         across(half, 0, 0)
+    started()
     for there in NEAR_FIRST:
         for half in both:
             arrive(half, 0, 0, there)
@@ -156,7 +181,7 @@
     def settle(chips):
         for half in both:
             for chip in chips:
-                first, second = chip[::-1] if HALF_AXES[half][0] == "kv_1" else chip
+                first, second = chip[::-1] if axes_of(half)[0] == "kv_1" else chip
                 arrive(half, "across", first, second)
 
     def pass_on(firsts, theres):
@@ -166,13 +191,18 @@
                     arrive(half, 1, first, there)
                     across(half, first, there)
 
-    ready = ready or (lambda group: None)
-    settle(IN_LINE)
-    ready(0)
+    if eager:
+        settle(IN_LINE)
+        ready(0)
     pass_on((1, 3), (1, 3))
-    ready(1)
+    if eager:
+        ready(1)
     pass_on((1, 3), (2,))
     pass_on((2,), (1, 3, 2))
+    if not eager:
+        settle(IN_LINE)
+        ready(0)
+        ready(1)
     settle(EARLY)
     ready(2)
     ready(3)
@@ -180,15 +210,11 @@
     ready(4)
 
 
-def axes_chip(half, first, second):
-    return (second, first) if HALF_AXES[half][0] == "kv_1" else (first, second)
-
-
 def add_up(wire, halves, value, last_out, last_in):
     copies = {}
-    sums = [None, None]
+    sums = [None] * len(halves)
     for turn, second in enumerate(FAR_FIRST):
-        for half in (0, 1):
+        for half in range(len(halves)):
             count = halves[half][1]
             result = value(turn, half)
             if second == 0:
@@ -198,20 +224,21 @@
             copies[half, turn] = wire.send(
                 last_out.at[half, turn, pl.ds(0, count), :],
                 last_in.at[half, turn, pl.ds(0, count), :],
-                HALF_AXES[half][1],
+                axes_of(half)[1],
                 second,
             )
     for turn in (1, 2, 0):
-        for half in (0, 1):
+        for half in range(len(halves)):
             copies[half, turn].wait_recv()
             sums[half] += last_in[half, turn, pl.ds(0, halves[half][1]), :].astype(F32)
     return sums
 
 
 def scatter_direct(wire, rows, term, between, buffers):
-    halves = halves_of(rows)
+    halves = pieces_of(rows)
     early_out, early_in, last_out, last_in = buffers
     copies = {}
+    keep = len(wire.sent)
     for turn, second in enumerate(FAR_FIRST):
         for way, step in enumerate(STEPS):
             for half in (0, 1):
@@ -222,10 +249,12 @@
                 copies[half, turn, way] = wire.send(
                     early_out.at[half, turn, way, pl.ds(0, count), :],
                     early_in.at[half, turn, way, pl.ds(0, count), :],
-                    HALF_AXES[half][0],
+                    axes_of(half)[0],
                     step,
                 )
         between(turn)
+
+    wire.finish(keep)
 
     def value(turn, half):
         start, count, _ = halves[half]
@@ -238,16 +267,17 @@
     return add_up(wire, halves, value, last_out, last_in)
 
 
-def scatter_relayed(wire, rows, term, buffers):
-    halves = halves_of(rows)
+def scatter_relayed(wire, halves, term, before, buffers):
     early_out, early_in, late_out, late_in, last_out, last_in = buffers
     copies = {}
+    keep = len(wire.sent)
 
     def parts(half):
         _, count, cut = halves[half]
         return ((0, cut, 1), (cut, count - cut, 3))
 
-    for half in (0, 1):
+    for half in range(len(halves)):
+        before(half)
         for turn, second in enumerate(FAR_FIRST):
             start, count, _ = halves[half]
             early_out[half, turn, pl.ds(0, count), :] = term(
@@ -257,11 +287,13 @@
                 copies["early", half, turn, step] = wire.send(
                     early_out.at[half, turn, pl.ds(at, length), :],
                     early_in.at[half, turn, pl.ds(at, length), :],
-                    HALF_AXES[half][0],
+                    axes_of(half)[0],
                     step,
+                    cross=False,
                 )
+    wire.finish(keep)
     for turn, second in enumerate(FAR_FIRST):
-        for half in (0, 1):
+        for half in range(len(halves)):
             start, count, _ = halves[half]
             for way, (at, length, step) in enumerate(parts(half)):
                 near = axes_chip(half, step, second)
@@ -277,7 +309,7 @@
                 copies["late", half, turn, way] = wire.send(
                     late_out.at[half, turn, way, pl.ds(0, count), :],
                     late_in.at[half, turn, way, pl.ds(0, count), :],
-                    HALF_AXES[half][0],
+                    axes_of(half)[0],
                     step,
                 )
 
@@ -292,12 +324,12 @@
     return add_up(wire, halves, value, last_out, last_in)
 
 
-def scatter_buffers(rows, relayed):
-    half = halves_of(rows)[0][1]
-    first = [(2, RING), (2, RING, 2)] if relayed else [(2, RING, len(STEPS))]
+def scatter_buffers(pieces, relayed):
+    number, half = len(pieces), pieces[0][1]
+    first = [(RING,), (RING, 2)] if relayed else [(RING, len(STEPS))]
     return [
-        pltpu.VMEM((*lead, half, LANES), BF16)
-        for lead in (*first, (2, RING))
+        pltpu.VMEM((number, *lead, half, LANES), BF16)
+        for lead in (*first, (RING,))
         for _ in (0, 1)
     ]
 
@@ -314,22 +346,34 @@
         pltpu.make_async_copy(
             up_hbm.at[:, columns], wide.at[pl.ds(half, hidden), here], sems.at[1]
         ).start()
-    for at, (along_0, along_1) in enumerate(CHIP_ORDER):
-        for other in (0, 1):
-            columns = pl.ds(
-                pl.multiple_of(block_of(place, along_0, along_1, other) * LANES, LANES), LANES
-            )
-            pltpu.make_async_copy(
-                down_hbm.at[:, columns],
-                down.at[at // 2, :, pl.ds((at % 2 * 2 + other) * LANES, LANES)],
-                sems.at[2],
-            ).start()
+    for at, chip in enumerate(CHIP_ORDER):
+        pltpu.make_async_copy(
+            down_hbm.at[:, columns_of(place, chip, 0)],
+            down.at[pl.ds(0, hidden), pl.ds(at * LANES, LANES)],
+            sems.at[2],
+        ).start()
+
+
+def columns_of(place, chip, core):
+    return pl.ds(pl.multiple_of(block_of(place, *chip, core) * LANES, LANES), LANES)
 
 
 def feed_forward(
-    place, wire, held, gain, gate_hbm, up_hbm, down_hbm, wide, down, sems, scratch, buffers
+    place,
+    wire,
+    held,
+    gain,
+    gate_hbm,
+    up_hbm,
+    down_hbm,
+    wide,
+    down,
+    sems,
+    scratch,
+    buffers,
+    after_swap=lambda: None,
 ):
-    scaled, squares, gains, acc, own, pair_out, pair_in = scratch
+    scaled, squares, gains, acc, own, units = scratch
     hidden, half = (gate_hbm.shape[0], wide.shape[0] // 2)
     rows, width = scaled.shape
     squares[...] = jnp.zeros_like(squares)
@@ -338,17 +382,16 @@
 
     def scale(block, carry):
         entry = held[block].astype(F32)
-        squares[...] += entry * entry
         scaled[:, pl.ds(pl.multiple_of(block * LANES, LANES), LANES)] = (
             entry * gains[pl.ds(block, 1), :]
         ).astype(BF16)
-        return carry
+        return carry + entry * entry
 
     def ready(group):
         with jax.named_scope("scale_and_product"):
             first = sum(len(blocks) for blocks in GROUPS[:group])
             last = first + len(GROUPS[group])
-            lax.fori_loop(first, last, scale, 0)
+            squares[...] = lax.fori_loop(first, last, scale, squares[...])
             if group == 0:
                 pltpu.make_async_copy(gate_hbm, wide.at[pl.ds(0, hidden), :], sems.at[0]).wait()
                 pltpu.make_async_copy(up_hbm, wide.at[pl.ds(half, hidden), :], sems.at[1]).wait()
@@ -361,51 +404,70 @@
             )
             acc[...] = part if group == 0 else acc[...] + part
 
+    def started():
+        for at, chip in enumerate(CHIP_ORDER):
+            down_copies.append(
+                wire.send(
+                    down_hbm.at[:, columns_of(place, chip, 1)],
+                    down.at[pl.ds(half, hidden), pl.ds(at * LANES, LANES)],
+                    "tp",
+                    1,
+                )
+            )
+
+    down_copies = []
     with jax.named_scope("gather_features"):
-        gather(wire, held, ready)
+        gather(wire, held, ready, True, started)
     with jax.named_scope("hidden"):
         row_scale = lax.rsqrt(jnp.sum(squares[...], axis=1, keepdims=True) / width + epsilon)
-        gate = row_scale * acc[:, :hidden]
-        up = row_scale * acc[:, half : half + hidden]
-        units = (gate / (1.0 + jnp.exp(-gate)) * up).astype(BF16)
-        pltpu.make_async_copy(down, down, sems.at[2]).wait()
-    pairs = CHIPS // 2
-    first = wire.take(pairs)
-
-    def pair_copy(at):
-        part = pl.ds(2 * at, 2)
-        return wire.make(pair_out.at[part], pair_in.at[part], "tp", 1, first + at)
-
-    done = [0]
-
-    def project(until):
+        gate = row_scale * acc[:, :half]
+        up = row_scale * acc[:, half:]
+        units[:, pl.ds(0, half)] = (gate / (1.0 + jnp.exp(-gate)) * up).astype(BF16)
+        swap = wire.send(
+            units.at[:, pl.ds(0, half)], units.at[:, pl.ds(half, half)], "tp", 1
+        )
+        after_swap()
+        arrived = down.at[pl.ds(0, hidden), :]
+        pltpu.make_async_copy(arrived, arrived, sems.at[2]).wait()
+
+    def product(first, last, begin, count):
+        chips = pl.ds(first * LANES, (last - first) * LANES)
+        return jnp.dot(
+            units[:, pl.ds(begin, count)],
+            down[pl.ds(begin, count), chips],
+            preferred_element_type=F32,
+        )
+
+    def project(first, last):
         with jax.named_scope("down"):
-            for at in range(done[0], until):
-                result = jnp.dot(units, down[at], preferred_element_type=F32)
-                for which in (0, 1):
-                    at_lane = 2 * which * LANES
-                    own[2 * at + which] = result[:, at_lane : at_lane + LANES]
-                    pair_out[2 * at + which] = result[
-                        :, at_lane + LANES : at_lane + 2 * LANES
-                    ].astype(BF16)
-                pair_copy(at).start()
-            done[0] = max(done[0], until)
-
-    arrived = set()
+            result = product(first, last, 0, 2 * half)
+            for at in range(first, last):
+                own[at] = result[:, (at - first) * LANES : (at - first + 1) * LANES]
+
+    ends = (5, 9, 13, CHIPS)
+    with jax.named_scope("down_first"):
+        kept = product(0, ends[0], 0, half)
+        for at in range(ends[0]):
+            own[at] = kept[:, at * LANES : (at + 1) * LANES]
+        for copy in down_copies:
+            copy.wait_recv()
+        swap.wait_recv()
+        kept = product(0, ends[0], half, half)
+        for at in range(ends[0]):
+            own[at] += kept[:, at * LANES : (at + 1) * LANES]
 
     def term(chip, start, count):
-        at = POSITION[chip]
-        if at // 2 not in arrived:
-            arrived.add(at // 2)
-            pair_copy(at // 2).wait_recv()
-        return own[at, pl.ds(start, count), :] + pair_in[at, pl.ds(start, count), :].astype(F32)
-
-    project(4)
+        return own[POSITION[chip], pl.ds(start, count), :]
+
+    def between(turn):
+        if turn == 0:
+            project(ends[0], ends[1])
+        elif turn == 1:
+            project(ends[1], ends[2])
+            project(ends[2], ends[3])
+
     with jax.named_scope("scatter_features"):
-        sums = scatter_direct(
-            wire, rows, term, lambda turn: project((5, 8, 8, 8)[turn]), buffers
-        )
-    wire.sent += [pair_copy(at) for at in range(pairs)]
+        sums = scatter_direct(wire, rows, term, between, buffers)
     return sums
 
 
@@ -414,23 +476,24 @@
     return [
         pltpu.VMEM((BLOCKS, rows, LANES), BF16),
         pltpu.VMEM((2 * half, width), BF16),
-        pltpu.VMEM((CHIPS // 2, hidden, 4 * LANES), BF16),
+        pltpu.VMEM((2 * half, CHIPS * LANES), BF16),
         pltpu.SemaphoreType.DMA((10,)),
         pltpu.VMEM((rows, width), BF16),
         pltpu.VMEM((rows, LANES), F32),
         pltpu.VMEM((BLOCKS, LANES), F32),
         pltpu.VMEM((rows, 2 * half), F32),
         pltpu.VMEM((CHIPS, rows, LANES), F32),
-        pltpu.VMEM((CHIPS, rows, LANES), BF16),
-        pltpu.VMEM((CHIPS, rows, LANES), BF16),
-        *scatter_buffers(rows, False),
+        pltpu.VMEM((rows, 2 * half), BF16),
+        *scatter_buffers(pieces_of(rows), False),
     ]
 
 
-def clear_padding(wide, hidden):
+def clear_padding(wide, down, hidden):
     half = wide.shape[0] // 2
-    for start in (hidden, half + hidden):
-        wide[pl.ds(start, half - hidden), :] = jnp.zeros((half - hidden, wide.shape[1]), BF16)
+    for array in (wide, down):
+        for start in (hidden, half + hidden):
+            rest = pl.ds(start, half - hidden)
+            array[rest, :] = jnp.zeros((half - hidden, array.shape[1]), BF16)
 
 
 def first_kernel(
@@ -457,12 +520,11 @@
     gains,
     acc,
     own,
-    pair_out,
-    pair_in,
+    units,
     *rest,
 ):
     buffers, own_refs, wide_buffers = (rest[:4], rest[4:13], rest[13:])
-    low, high, share, ordered, wide_own, wide_out, wide_in, first_gain, mix_gain = own_refs
+    low, high, share, ordered, rows_out, rows_in, wide_own, first_gain, mix_gain = own_refs
     place = own_place()
     wire = Wire(place, send_sems, recv_sems)
     own_tokens = pltpu.make_async_copy(tokens, held.at[0], sems.at[3])
@@ -478,21 +540,29 @@
             lambda: load_feed_forward(place, gate_hbm, up_hbm, down_hbm, wide, down, sems)
         )
     own_tokens.wait()
-    width = query_hbm.shape[1]
+    share_width, width = query_hbm.shape
+    weights = (
+        (query_hbm, low, 0),
+        (forget_hbm, low, width),
+        (input_hbm, high, 0),
+        (outgate_hbm, high, width),
+    )
     loads = [
-        pltpu.make_async_copy(source, target.at[:, pl.ds(at, width)], sems.at[4 + index])
-        for index, (source, target, at) in enumerate(
-            (
-                (query_hbm, low, 0),
-                (forget_hbm, low, width),
-                (input_hbm, high, 0),
-                (outgate_hbm, high, width),
-            )
+        pltpu.make_async_copy(
+            source, target.at[pl.ds(0, share_width), pl.ds(at, width)], sems.at[4 + index]
         )
+        for index, (source, target, at) in enumerate(weights)
     ]
+    weight_copies = []
+
+    def share_weights():
+        for source, target, at in weights:
+            there = target.at[pl.ds(share_width, share_width), pl.ds(at, width)]
+            weight_copies.append(wire.send(source, there, "tp", 1))
+
     for load in loads:
         load.start()
-    clear_padding(wide, gate_hbm.shape[0])
+    clear_padding(wide, down, gate_hbm.shape[0])
     for load in gain_loads:
         load.wait()
     sums = feed_forward(
@@ -506,40 +576,50 @@
         wide,
         down,
         sems,
-        (scaled, squares, gains, acc, own, pair_out, pair_in),
+        (scaled, squares, gains, acc, own, units),
         buffers,
+        share_weights,
     )
     rows = share.shape[0]
-    for (start, count, _), value in zip(halves_of(rows), sums):
+    for (start, count, _), value in zip(pieces_of(rows), sums):
         part = pl.ds(start, count)
         mixed = (held[0, part, :].astype(F32) + 0.5 * value).astype(BF16)
         mixer_share[part, :] = mixed
         share[part, :] = mixed.astype(F32)
     seqs = rows // BLOCKS
     for block in range(BLOCKS):
-        index = block_of(place, block // (2 * RING), block // 2 % RING, block % 2)
+        chip = (block // RING % RING, block % RING)
+        index = block_of(place, *chip, block // CHIPS)
         ordered[pl.ds(block * seqs, seqs), :] = share[
             pl.ds(pl.multiple_of(index * seqs, seqs), seqs), :
         ]
-    entry = ordered[...]
-    index = block_of(place, 0, 0, 0)
-    mix_scaled = (entry * mix_gain[pl.ds(index, 1), :]).astype(BF16)
-    square_sum = jnp.broadcast_to(jnp.sum(entry * entry, axis=1, keepdims=True), entry.shape)
+    side = rows // 2
+    rows_out[...] = ordered[pl.ds(side, side), :].astype(BF16)
+    swap = wire.send(rows_out, rows_in, "tp", 1)
     for load in loads:
         load.wait()
+    for copy in weight_copies:
+        copy.wait_recv()
+    swap.wait_recv()
+    entries = (ordered[pl.ds(0, side), :], rows_in[...].astype(F32))
+    mix_scaled = jnp.concatenate(
+        [
+            entry * mix_gain[pl.ds(block_of(place, 0, 0, core), 1), :]
+            for core, entry in enumerate(entries)
+        ],
+        axis=1,
+    ).astype(BF16)
+    square_sum = sum(jnp.sum(entry * entry, axis=1, keepdims=True) for entry in entries)
+    square_sum = jnp.broadcast_to(square_sum, entries[0].shape)
 
     def keep(at, lower, upper):
-        pair = jnp.concatenate(
-            [lower.reshape(BLOCKS, seqs, LANES), upper.reshape(BLOCKS, seqs, LANES)], axis=1
-        ).reshape(RING, RING, 2, 2 * seqs, LANES)
-        wide_own[:, :, pl.ds(at, 2 * seqs), :] = pair[:, :, 0]
-        wide_out[:, :, pl.ds(at, 2 * seqs), :] = pair[:, :, 1].astype(BF16)
+        both = [part.reshape(RING, RING, seqs, LANES) for part in (lower, upper)]
+        wide_own[:, :, pl.ds(at, 2 * seqs), :] = jnp.concatenate(both, axis=2)
 
     tile = 2 * seqs
     wide_rows = wide_own.shape[2]
-    wide_halves = halves_of(wide_rows)
+    wide_halves = pieces_of(wide_rows, WIDE_PIECES)
     columns = low.shape[1] // LANES
-    copies = {}
 
     def project(steps):
         with jax.named_scope("project"):
@@ -551,39 +631,21 @@
                     lanes = slice(which * LANES, (which + 1) * LANES)
                     keep((2 * step + which) * tile, lower[:, lanes], upper[:, lanes])
 
-    def across(half, first):
-        part = pl.ds(*wide_halves[half][:2])
-        chips = (slice(None), first) if HALF_AXES[half][0] == "kv_1" else (first, slice(None))
-        copies[half, first] = wire.send(
-            wide_out.at[(*chips, part, slice(None))],
-            wide_in.at[(*chips, part, slice(None))],
-            "tp",
-            1,
-        )
-
-    first_steps = -(-wide_halves[0][1] // (2 * tile))
-    project(range(first_steps))
-    across(0, 2)
-    project(range(first_steps, columns // 2))
-    keep(columns * tile, square_sum, jnp.zeros_like(square_sum))
-    across(1, 2)
-    for first in (1, 3, 0):
-        for half in (0, 1):
-            across(half, first)
-    arrived = set()
+    ends = [
+        min(-(-(start + count) // (2 * tile)), columns // 2) for start, count, _ in wide_halves
+    ]
+
+    def before(piece):
+        project(range(ends[piece - 1] if piece else 0, ends[piece]))
+        if piece + 1 == len(wide_halves):
+            keep(columns * tile, square_sum, jnp.zeros_like(square_sum))
 
     def term(chip, start, count):
-        half = 0 if start < wide_halves[1][0] else 1
-        first = chip[1] if HALF_AXES[half][0] == "kv_1" else chip[0]
-        if (half, first) not in arrived:
-            arrived.add((half, first))
-            copies[half, first].wait_recv()
-        part = pl.ds(start, count)
-        return wide_own[(*chip, part)] + wide_in[(*chip, part)].astype(F32)
+        return wide_own[(*chip, pl.ds(start, count))]
 
     with jax.named_scope("scatter_wide"):
-        sums = scatter_relayed(wire, wide_rows, term, wide_buffers)
-    for (start, count, _), value in zip(halves_of(wide_rows), sums):
+        sums = scatter_relayed(wire, wide_halves, term, before, wide_buffers)
+    for (start, count, _), value in zip(wide_halves, sums):
         projected[pl.ds(start, count), :] = value
     with jax.named_scope("finish"):
         wire.finish()
@@ -628,7 +690,8 @@
         for seq in range(seqs):
             kept = spread[:keys, seq * values : (seq + 1) * values]
             asked = spread[keys:, seq * values : (seq + 1) * values]
-            after = kept * state[seq, head] + (1.0 - kept) * entering[seq : seq + 1, :]
+            fresh = entering[seq : seq + 1, :]
+            after = fresh + kept * (state[seq, head] - fresh)
             held[head, seq] = after
             readouts.append(jnp.sum(after * asked, axis=0, keepdims=True))
         writes[head].start()
@@ -665,8 +728,7 @@
     gains,
     acc,
     own,
-    pair_out,
-    pair_in,
+    units,
     *rest,
 ):
     buffers, (mixed, output, update, mixer_share, second_gain) = rest[:4], rest[4:]
@@ -691,33 +753,40 @@
         wire.greet(
             lambda: load_feed_forward(place, gate_hbm, up_hbm, down_hbm, wide, down, sems)
         )
-    clear_padding(wide, gate_hbm.shape[0])
-    with jax.named_scope("gather_mixed"):
-        gather(wire, mixed)
-    for load in loads:
-        load.wait()
+    clear_padding(wide, down, gate_hbm.shape[0])
     rows = update.shape[0]
     seqs = rows // BLOCKS
     tile = 2 * seqs
-    total = None
-    for step in range(depth // (2 * LANES)):
-        pieces = [
-            mixed[:, pl.ds((2 * step + which) * tile, tile), :].reshape(
-                BLOCKS * tile, LANES
-            )
-            for which in (0, 1)
-        ]
-        product = jnp.dot(
-            jnp.concatenate(pieces, axis=1),
-            output[pl.ds(step * 2 * LANES, 2 * LANES), :],
-            preferred_element_type=F32,
-        )
-        total = product if total is None else total + product
-    total = total.reshape(BLOCKS, tile, 2 * LANES)
-    total = total[:, :seqs, :LANES] + total[:, seqs:, LANES:]
-    for block in range(BLOCKS):
-        index = block_of(place, *ORDER[block])
-        update[pl.ds(pl.multiple_of(index * seqs, seqs), seqs), :] = total[block]
+
+    def project(group):
+        with jax.named_scope("output"):
+            if group == 0:
+                for load in loads:
+                    load.wait()
+            first = sum(len(blocks) for blocks in GROUPS[:group])
+            number = len(GROUPS[group])
+            total = None
+            for step in range(depth // (2 * LANES)):
+                pieces = [
+                    mixed[
+                        pl.ds(first, number), pl.ds((2 * step + which) * tile, tile), :
+                    ].reshape(number * tile, LANES)
+                    for which in (0, 1)
+                ]
+                product = jnp.dot(
+                    jnp.concatenate(pieces, axis=1),
+                    output[pl.ds(step * 2 * LANES, 2 * LANES), :],
+                    preferred_element_type=F32,
+                )
+                total = product if total is None else total + product
+            total = total.reshape(number, tile, 2 * LANES)
+            total = total[:, :seqs, :LANES] + total[:, seqs:, LANES:]
+            for at, block in enumerate(GROUPS[group]):
+                index = block_of(place, *block)
+                update[pl.ds(pl.multiple_of(index * seqs, seqs), seqs), :] = total[at]
+
+    with jax.named_scope("gather_mixed"):
+        gather(wire, mixed, project, False)
     held[0] = (mixer_share[...].astype(F32) + update[...]).astype(BF16)
     sums = feed_forward(
         place,
@@ -730,10 +799,10 @@
         wide,
         down,
         sems,
-        (scaled, squares, gains, acc, own, pair_out, pair_in),
+        (scaled, squares, gains, acc, own, units),
         buffers,
     )
-    for (start, count, _), value in zip(halves_of(rows), sums):
+    for (start, count, _), value in zip(pieces_of(rows), sums):
         part = pl.ds(start, count)
         layer_out[part, :] = (held[0, part, :].astype(F32) + 0.5 * value).astype(BF16)
     with jax.named_scope("finish"):
@@ -787,19 +856,19 @@
         in_specs=in_space(*(HBM,) * 10),
         out_specs=in_space(VMEM, VMEM),
         scratch_shapes=[
-            pltpu.SemaphoreType.DMA((192,)),
-            pltpu.SemaphoreType.DMA((192,)),
+            pltpu.SemaphoreType.DMA((208,)),
+            pltpu.SemaphoreType.DMA((208,)),
             *feed_forward_scratch(rows, full_width, hidden),
-            pltpu.VMEM((share, 2 * heads * keys), BF16),
-            pltpu.VMEM((share, 2 * heads * values), BF16),
+            pltpu.VMEM((2 * share, 2 * heads * keys), BF16),
+            pltpu.VMEM((2 * share, 2 * heads * values), BF16),
             pltpu.VMEM((rows, LANES), F32),
             pltpu.VMEM((rows, LANES), F32),
+            pltpu.VMEM((rows // 2, LANES), BF16),
+            pltpu.VMEM((rows // 2, LANES), BF16),
             pltpu.VMEM((RING, RING, wide_rows, LANES), F32),
-            pltpu.VMEM((RING, RING, wide_rows, LANES), BF16),
-            pltpu.VMEM((RING, RING, wide_rows, LANES), BF16),
             pltpu.VMEM(by_block, F32),
             pltpu.VMEM(by_block, F32),
-            *scatter_buffers(wide_rows, True),
+            *scatter_buffers(pieces_of(wide_rows, WIDE_PIECES), True),
         ],
         compiler_params=kernel_params(0, 44),
     )(
@@ -841,8 +910,8 @@
         in_specs=in_space(VMEM, *(HBM,) * 6),
         out_specs=pl.BlockSpec(memory_space=VMEM),
         scratch_shapes=[
-            pltpu.SemaphoreType.DMA((224,)),
-            pltpu.SemaphoreType.DMA((224,)),
+            pltpu.SemaphoreType.DMA((176,)),
+            pltpu.SemaphoreType.DMA((176,)),
             *feed_forward_scratch(rows, full_width, hidden),
             pltpu.VMEM((BLOCKS, heads * seqs, LANES), BF16),
             pltpu.VMEM((heads * values // 2, 2 * LANES), BF16),

time: 96.7 us -> 93.4 us (0.966)
  Pallas kernels: 94.4 us -> 91.7 us
    pallas_call x1, Pallas kernels: 51.5 us -> 49.6 us  [per_device(): pl.pallas_call(first_kernel, name='first_block', out_shape=(jax.ShapeDtyp...]
where the time goes in v4:
time: 93.4 us; the launch traced here: 93 us
  Pallas kernels  91.7 us (98%)
    pallas_call x1, Pallas kernels, per_device(): pl.pallas_call(first_kernel, name='first_block', out_shape=(jax.ShapeDtyp...  49.6 us
    pallas_call x1, Pallas kernels, per_device(): pl.pallas_call(second_kernel, name='second_block', out_shape=jax.ShapeDty...  38.3 us
    pallas_call x1, Pallas kernels, per_device(): pl.pallas_call(lambda *refs: state_kernel(full_width, *refs), name='state...  3.77 us

profile of v4, /device:TPU:0, one launch (start us, length us, event | category | flops | bytes accessed | tf_op | source)
XLA Modules:
  0.0 93.0 jit_solution(3445897111389071973)
XLA Ops:
  0.6 0.0 copy-start
  0.6 0.0 copy-start.1
  0.7 0.0 copy-start.2
  0.7 49.6 %first_block.1 = (f32[528,128]{1,0:T(8,128)S(1)}, bf16[256,128]{1,0:T(8,128)(2,1)S(1)}) custom-call(bf16[256,128]{1,0:T(8,128)(2,1)} %tokens.1, bf16[352,4096]{1,0:T(8,128)(2,1)} %bitcast.11, bf16[352,4096]{1,0:T(8,128)(2,1)} %bitcast.12, bf16[352,4096]{1,0:T(8,128)(2,1)} %down_hbm.2, f32[32,128]{1,0:T(8,128)} %bitcast.15, f32[32,128]{1,0:T(8,128)} %bitcast.16, ...), custom_call_target="tpu_custom_call" | custom-call | tf_op jit(solution)/shard_map/first_block/pallas_call | solution.py:849
  50.3 0.0 copy-done
  50.3 0.0 copy-done.1
  50.3 0.0 copy-done.2
  50.3 3.8 %state_update.1 = (f32[8,16,128,128]{3,2,1,0:T(8,128)}, f32[128,128]{1,0:T(8,128)S(1)}) custom-call(f32[528,128]{1,0:T(8,128)S(1)} %get-tuple-element.6.refs_0_, f32[16,128]{1,0:T(8,128)S(1)} %bitcast.9, f32[1,128]{1,0:T(1,128)S(1)} %bitcast.10, f32[8,16,128,128]{3,2,1,0:T(8,128)S(1)} %copy-done), custom_call_target="tpu_custom_call" | custom-call | tf_op jit(solution)/shard_map/state_update/pallas_call | solution.py:886
  54.1 38.3 %second_block.1 = bf16[256,128]{1,0:T(8,128)(2,1)S(1)} custom-call(f32[128,128]{1,0:T(8,128)S(1)} %get-tuple-element.7.mixer_out, bf16[256,128]{1,0:T(8,128)(2,1)S(1)} %get-tuple-element.8.share_hbm, bf16[2048,128]{1,0:T(8,128)(2,1)} %output_hbm.1, bf16[352,4096]{1,0:T(8,128)(2,1)} %bitcast.13, bf16[352,4096]{1,0:T(8,128)(2,1)} %bitcast.14, ...), custom_call_target="tpu_custom_call" | custom-call | tf_op jit(solution)/shard_map/second_block/pallas_call | solution.py:906
  92.4 0.6 copy.21
Async XLA Ops:
  0.6 49.6 %copy-start = (f32[8,16,128,128]{3,2,1,0:T(8,128)S(1)}, f32[8,16,128,128]{3,2,1,0:T(8,128)}, u32[]{:S(2)}) copy-start(f32[8,16,128,128]{3,2,1,0:T(8,128)} %refs_3_.1) | copy-start | bytes 25165828
  0.6 49.6 %copy-start.1 = (f32[2048]{0:T(1024)S(1)}, f32[2048]{0:T(1024)}, u32[]{:S(2)}) copy-start(f32[2048]{0:T(1024)} %param.29) | copy-start | bytes 24580
  0.7 49.6 %copy-start.2 = (f32[128]{0:T(128)S(1)}, f32[128]{0:T(128)}, u32[]{:S(2)}) copy-start(f32[128]{0:T(128)} %param.30) | copy-start | bytes 1540

commit v5 on v4

--- a/solution.py
+++ b/solution.py
@@ -20,10 +20,7 @@
 CHIPS = RING * RING
 WIDE_PIECES = 4
 BLOCKS = 2 * CHIPS
-NEAR = (
-    *((axis, step, 0) for axis in ("kv_0", "kv_1") for step in (2, 1, 3)),
-    ("tp", 1, 0),
-)
+NEAR = tuple((axis, step) for axis in ("kv_0", "kv_1") for step in (2, 1, 3)) + (("tp", 1),)
 HALF_AXES = (("kv_1", "kv_0"), ("kv_0", "kv_1"))
 FAR_FIRST = (2, 1, 3, 0)
 NEAR_FIRST = (1, 3, 2)
@@ -47,10 +44,6 @@
 POSITION = {chip: place for place, chip in enumerate(CHIP_ORDER)}
 
 
-def crosses(chip):
-    return 0
-
-
 def own_place():
     return (lax.axis_index("kv_0"), lax.axis_index("kv_1"), lax.axis_index("tp"))
 
@@ -67,53 +60,58 @@
 class Wire:
     def __init__(self, place, send_sems, recv_sems):
         at_0, at_1, core = place
+        self.core = core
         self.place = {"kv_0": (at_0, RING), "kv_1": (at_1, RING), "tp": (core, 2)}
         self.send_sems, self.recv_sems = send_sems, recv_sems
-        self.used = 0
-        self.sent = []
-
-    def near(self, axis, step, cross):
+        self.sends = self.receives = 0
+        self.owed = []
+
+    def near(self, axis, step):
         at, size = self.place[axis]
-        there = {axis: lax.rem(at + step, size)}
-        if cross:
-            there["tp"] = 1 - self.place["tp"][0]
-        return there
+        return {axis: lax.rem(at + step, size)}
 
     def greet(self, meanwhile):
         barrier = pltpu.get_barrier_semaphore()
-        for axis, step, cross in NEAR:
+        for axis, step in NEAR:
             pl.semaphore_signal(
-                barrier, inc=1, device_id=self.near(axis, step, cross), device_id_type=MESH
+                barrier, inc=1, device_id=self.near(axis, step), device_id_type=MESH
             )
         meanwhile()
         pl.semaphore_wait(barrier, len(NEAR))
 
-    def take(self, count):
-        first = self.used
-        self.used += count
-        return first
-
-    def make(self, source, target, axis, step, slot, cross=0):
+    def sender(self, ref):
+        self.sends += 1
+        self.owed.append((self.sends - 1, ref))
+        return self.sends - 1
+
+    def receiver(self):
+        self.receives += 1
+        return self.receives - 1
+
+    def prepare(self, source, target, axis, step, send, receive):
         return pltpu.make_async_remote_copy(
             src_ref=source,
             dst_ref=target,
-            send_sem=self.send_sems.at[slot],
-            recv_sem=self.recv_sems.at[slot],
-            device_id=self.near(axis, step, cross),
+            send_sem=self.send_sems.at[send],
+            recv_sem=self.recv_sems.at[receive],
+            device_id=self.near(axis, step),
             device_id_type=MESH,
         )
 
-    def send(self, source, target, axis, step, cross=None):
-        cross = 0
-        copy = self.make(source, target, axis, step, self.take(1), cross)
+    def send(self, source, target, axis, step, send=None, receive=None):
+        send = self.sender(source) if send is None else send
+        receive = self.receiver() if receive is None else receive
+        copy = self.prepare(source, target, axis, step, send, receive)
         copy.start()
-        self.sent.append(copy)
         return copy
 
+    def receive(self, receive, ref):
+        pltpu.make_async_copy(ref, ref, self.recv_sems.at[receive]).wait()
+
     def finish(self, count=None):
-        for copy in self.sent[:count]:
-            copy.wait_send()
-        self.sent = self.sent[count:] if count is not None else []
+        for send, ref in self.owed[:count]:
+            pltpu.make_async_copy(ref, ref, self.send_sems.at[send]).wait()
+        self.owed = self.owed[count:] if count is not None else []
 
 
 def pieces_of(rows, number=2):
@@ -133,6 +131,8 @@
 def gather(wire, held, ready, eager, started=lambda: None):
     halves = pieces_of(held.shape[1])
     copies = {}
+    send = wire.sender(held.at[pl.ds(0, BLOCKS - 1)])
+    crossing = {chips: wire.receiver() for chips in (IN_LINE, EARLY, LATE)}
 
     def view(half, first, second, core):
         start, rows, _ = halves[half]
@@ -145,17 +145,21 @@
             chip = (there, 0) if stage == 0 else (first, there)
             source = (0, 0) if stage == 0 else (first, 0)
             copies[half, stage, first, there] = wire.send(
-                view(half, *source, crosses(source)),
-                view(half, *chip, crosses(chip)),
+                view(half, *source, 0),
+                view(half, *chip, 0),
                 axes_of(half)[stage],
                 step,
+                send,
             )
 
+    def crossed(half, first, second):
+        chip = axes_chip(half, first, second)
+        group = next(chips for chips in crossing if chip in chips)
+        source, target = (view(half, first, second, core) for core in (0, 1))
+        return wire.prepare(source, target, "tp", 1, send, crossing[group])
+
     def across(half, first, second):
-        core = crosses((first, second))
-        copies[half, "across", first, second] = wire.send(
-            view(half, first, second, core), view(half, first, second, 1 - core), "tp", 1
-        )
+        crossed(half, first, second).start()
 
     def arrive(half, stage, first, there):
         copies[half, stage, first, there].wait_recv()
@@ -179,40 +183,66 @@
             across(half, 0, there)
 
     def settle(chips):
-        for half in both:
-            for chip in chips:
-                first, second = chip[::-1] if axes_of(half)[0] == "kv_1" else chip
-                arrive(half, "across", first, second)
-
-    def pass_on(firsts, theres):
-        for first in firsts:
-            for there in theres:
-                for half in both:
-                    arrive(half, 1, first, there)
-                    across(half, first, there)
+        blocks = held.at[pl.ds(KEPT_AT[(*chips[0], 1)], len(chips))]
+        wire.receive(crossing[chips], blocks)
+
+    aside = [
+        (half, first, there)
+        for firsts, theres in (((1, 3), (1, 3)), ((1, 3), (2,)), ((2,), NEAR_FIRST))
+        for first in firsts
+        for there in theres
+        for half in both
+    ]
+    for half, first, there in aside:
+        copies[half, "across", first, there] = crossed(half, first, there)
+    early, late = aside[:8], aside[8:]
+
+    def pass_on(blocks):
+        for half, first, there in blocks:
+            arrive(half, 1, first, there)
+            copies[half, "across", first, there].start()
 
     if eager:
+        @pl.when(wire.core == 1)
+        def _():
+            pass_on(early)
+
         settle(IN_LINE)
         ready(0)
-    pass_on((1, 3), (1, 3))
-    if eager:
+
+        @pl.when(wire.core == 1)
+        def _():
+            pass_on(late)
+
+        @pl.when(wire.core == 0)
+        def _():
+            pass_on(early)
+
         ready(1)
-    pass_on((1, 3), (2,))
-    pass_on((2,), (1, 3, 2))
-    if not eager:
+        settle(EARLY)
+        ready(2)
+
+        @pl.when(wire.core == 0)
+        def _():
+            pass_on(late)
+
+    else:
+        pass_on(early + late)
         settle(IN_LINE)
         ready(0)
         ready(1)
-    settle(EARLY)
-    ready(2)
+        settle(EARLY)
+        ready(2)
     ready(3)
     settle(LATE)
     ready(4)
 
 
 def add_up(wire, halves, value, last_out, last_in):
-    copies = {}
     sums = [None] * len(halves)
+    rows = [pl.ds(0, count) for _, count, _ in halves]
+    sends = [wire.sender(last_out.at[half, pl.ds(0, 3), part]) for half, part in enumerate(rows)]
+    receives = [wire.receiver() for _ in halves]
     for turn, second in enumerate(FAR_FIRST):
         for half in range(len(halves)):
             count = halves[half][1]
@@ -221,15 +251,17 @@
                 sums[half] = result
                 continue
             last_out[half, turn, pl.ds(0, count), :] = result.astype(BF16)
-            copies[half, turn] = wire.send(
+            wire.send(
                 last_out.at[half, turn, pl.ds(0, count), :],
                 last_in.at[half, turn, pl.ds(0, count), :],
                 axes_of(half)[1],
                 second,
+                sends[half],
+                receives[half],
             )
-    for turn in (1, 2, 0):
-        for half in range(len(halves)):
-            copies[half, turn].wait_recv()
+    for half, part in enumerate(rows):
+        wire.receive(receives[half], last_in.at[half, pl.ds(0, 3), part])
+        for turn in (1, 2, 0):
             sums[half] += last_in[half, turn, pl.ds(0, halves[half][1]), :].astype(F32)
     return sums
 
@@ -237,8 +269,10 @@
 def scatter_direct(wire, rows, term, between, buffers):
     halves = pieces_of(rows)
     early_out, early_in, last_out, last_in = buffers
-    copies = {}
-    keep = len(wire.sent)
+    keep = len(wire.owed)
+    rows = [pl.ds(0, count) for _, count, _ in halves]
+    sends = [wire.sender(early_out.at[half, :, :, part]) for half, part in enumerate(rows)]
+    receives = [[wire.receiver() for _ in FAR_FIRST] for _ in halves]
     for turn, second in enumerate(FAR_FIRST):
         for way, step in enumerate(STEPS):
             for half in (0, 1):
@@ -246,11 +280,13 @@
                 early_out[half, turn, way, pl.ds(0, count), :] = term(
                     axes_chip(half, step, second), start, count
                 ).astype(BF16)
-                copies[half, turn, way] = wire.send(
+                wire.send(
                     early_out.at[half, turn, way, pl.ds(0, count), :],
                     early_in.at[half, turn, way, pl.ds(0, count), :],
                     axes_of(half)[0],
                     step,
+                    sends[half],
+                    receives[half][turn],
                 )
         between(turn)
 
@@ -259,8 +295,8 @@
     def value(turn, half):
         start, count, _ = halves[half]
         result = term(axes_chip(half, 0, FAR_FIRST[turn]), start, count)
+        wire.receive(receives[half][turn], early_in.at[half, turn, :, rows[half]])
         for way in range(len(STEPS)):
-            copies[half, turn, way].wait_recv()
             result += early_in[half, turn, way, pl.ds(0, count), :].astype(F32)
         return result
 
@@ -269,8 +305,13 @@
 
 def scatter_relayed(wire, halves, term, before, buffers):
     early_out, early_in, late_out, late_in, last_out, last_in = buffers
-    copies = {}
-    keep = len(wire.sent)
+    keep = len(wire.owed)
+    rows = [pl.ds(0, count) for _, count, _ in halves]
+    early_sends = [wire.sender(early_out.at[half, :, part]) for half, part in enumerate(rows)]
+    late_sends = [wire.sender(late_out.at[half, :, :, part]) for half, part in enumerate(rows)]
+    early_receives, late_receives = (
+        [[wire.receiver() for _ in FAR_FIRST] for _ in halves] for _ in (0, 1)
+    )
 
     def parts(half):
         _, count, cut = halves[half]
@@ -284,40 +325,43 @@
                 axes_chip(half, 2, second), start, count
             ).astype(BF16)
             for at, length, step in parts(half):
-                copies["early", half, turn, step] = wire.send(
+                wire.send(
                     early_out.at[half, turn, pl.ds(at, length), :],
                     early_in.at[half, turn, pl.ds(at, length), :],
                     axes_of(half)[0],
                     step,
-                    cross=False,
+                    early_sends[half],
+                    early_receives[half][turn],
                 )
     wire.finish(keep)
     for turn, second in enumerate(FAR_FIRST):
         for half in range(len(halves)):
             start, count, _ = halves[half]
+            wire.receive(early_receives[half][turn], early_in.at[half, turn, rows[half]])
             for way, (at, length, step) in enumerate(parts(half)):
                 near = axes_chip(half, step, second)
                 rest_at, rest = (length, count - length) if at == 0 else (0, at)
                 late_out[half, turn, way, pl.ds(rest_at, rest), :] = term(
                     near, start + rest_at, rest
                 ).astype(BF16)
-                copies["early", half, turn, step].wait_recv()
                 late_out[half, turn, way, pl.ds(at, length), :] = (
                     term(near, start + at, length)
                     + early_in[half, turn, pl.ds(at, length), :].astype(F32)
                 ).astype(BF16)
-                copies["late", half, turn, way] = wire.send(
+                wire.send(
                     late_out.at[half, turn, way, pl.ds(0, count), :],
                     late_in.at[half, turn, way, pl.ds(0, count), :],
                     axes_of(half)[0],
                     step,
+                    late_sends[half],
+                    late_receives[half][turn],
                 )
 
     def value(turn, half):
         start, count, _ = halves[half]
         result = term(axes_chip(half, 0, FAR_FIRST[turn]), start, count)
+        wire.receive(late_receives[half][turn], late_in.at[half, turn, :, rows[half]])
         for way in (0, 1):
-            copies["late", half, turn, way].wait_recv()
             result += late_in[half, turn, way, pl.ds(0, count), :].astype(F32)
         return result
 
@@ -405,17 +449,18 @@
             acc[...] = part if group == 0 else acc[...] + part
 
     def started():
+        send = wire.sender(others)
         for at, chip in enumerate(CHIP_ORDER):
-            down_copies.append(
-                wire.send(
-                    down_hbm.at[:, columns_of(place, chip, 1)],
-                    down.at[pl.ds(half, hidden), pl.ds(at * LANES, LANES)],
-                    "tp",
-                    1,
-                )
+            wire.send(
+                down_hbm.at[:, columns_of(place, chip, 1)],
+                down.at[pl.ds(half, hidden), pl.ds(at * LANES, LANES)],
+                "tp",
+                1,
+                send,
+                others_receive,
             )
 
-    down_copies = []
+    others, others_receive = down.at[pl.ds(half, hidden), :], wire.receiver()
     with jax.named_scope("gather_features"):
         gather(wire, held, ready, True, started)
     with jax.named_scope("hidden"):
@@ -449,8 +494,7 @@
         kept = product(0, ends[0], 0, half)
         for at in range(ends[0]):
             own[at] = kept[:, at * LANES : (at + 1) * LANES]
-        for copy in down_copies:
-            copy.wait_recv()
+        wire.receive(others_receive, others)
         swap.wait_recv()
         kept = product(0, ends[0], half, half)
         for at in range(ends[0]):
@@ -556,9 +600,10 @@
     weight_copies = []
 
     def share_weights():
+        send = wire.sender(low)
         for source, target, at in weights:
             there = target.at[pl.ds(share_width, share_width), pl.ds(at, width)]
-            weight_copies.append(wire.send(source, there, "tp", 1))
+            weight_copies.append(wire.send(source, there, "tp", 1, send))
 
     for load in loads:
         load.start()
@@ -649,6 +694,7 @@
         projected[pl.ds(start, count), :] = value
     with jax.named_scope("finish"):
         wire.finish()
+    assert (wire.sends, wire.receives) == (send_sems.shape[0], recv_sems.shape[0]), (wire.sends, wire.receives)
 
 
 def state_kernel(
@@ -807,6 +853,7 @@
         layer_out[part, :] = (held[0, part, :].astype(F32) + 0.5 * value).astype(BF16)
     with jax.named_scope("finish"):
         wire.finish()
+    assert (wire.sends, wire.receives) == (send_sems.shape[0], recv_sems.shape[0]), (wire.sends, wire.receives)
 
 
 def in_space(*spaces):
@@ -856,8 +903,8 @@
         in_specs=in_space(*(HBM,) * 10),
         out_specs=in_space(VMEM, VMEM),
         scratch_shapes=[
-            pltpu.SemaphoreType.DMA((208,)),
-            pltpu.SemaphoreType.DMA((208,)),
+            pltpu.SemaphoreType.DMA((21,)),
+            pltpu.SemaphoreType.DMA((86,)),
             *feed_forward_scratch(rows, full_width, hidden),
             pltpu.VMEM((2 * share, 2 * heads * keys), BF16),
             pltpu.VMEM((2 * share, 2 * heads * values), BF16),
@@ -910,8 +957,8 @@
         in_specs=in_space(VMEM, *(HBM,) * 6),
         out_specs=pl.BlockSpec(memory_space=VMEM),
         scratch_shapes=[
-            pltpu.SemaphoreType.DMA((176,)),
-            pltpu.SemaphoreType.DMA((176,)),
+            pltpu.SemaphoreType.DMA((8,)),
+            pltpu.SemaphoreType.DMA((78,)),
             *feed_forward_scratch(rows, full_width, hidden),
             pltpu.VMEM((BLOCKS, heads * seqs, LANES), BF16),
             pltpu.VMEM((heads * values // 2, 2 * LANES), BF16),

time: 93.4 us -> 88.1 us (0.943)
  Pallas kernels: 91.7 us -> 86.4 us
    pallas_call x1, Pallas kernels: 49.6 us -> 46.8 us  [per_device(): pl.pallas_call(first_kernel, name='first_block', out_shape=(jax.ShapeDtyp...]
    pallas_call x1, Pallas kernels: 38.3 us -> 35.8 us  [per_device(): pl.pallas_call(second_kernel, name='second_block', out_shape=jax.ShapeDty...]
where the time goes in v5:
time: 88.1 us; the launch traced here: 87.8 us
  Pallas kernels  86.4 us (98%)
    pallas_call x1, Pallas kernels, per_device(): pl.pallas_call(first_kernel, name='first_block', out_shape=(jax.ShapeDtyp...  46.8 us
    pallas_call x1, Pallas kernels, per_device(): pl.pallas_call(second_kernel, name='second_block', out_shape=jax.ShapeDty...  35.8 us
    pallas_call x1, Pallas kernels, per_device(): pl.pallas_call(lambda *refs: state_kernel(full_width, *refs), name='state...  3.77 us

profile of v5, /device:TPU:0, one launch (start us, length us, event | category | flops | bytes accessed | tf_op | source)
XLA Modules:
  0.0 87.8 jit_solution(8667939191689263133)
XLA Ops:
  0.6 0.0 copy-start
  0.6 0.0 copy-start.1
  0.7 0.0 copy-start.2
  0.7 46.8 %first_block.1 = (f32[528,128]{1,0:T(8,128)S(1)}, bf16[256,128]{1,0:T(8,128)(2,1)S(1)}) custom-call(bf16[256,128]{1,0:T(8,128)(2,1)} %tokens.1, bf16[352,4096]{1,0:T(8,128)(2,1)} %bitcast.11, bf16[352,4096]{1,0:T(8,128)(2,1)} %bitcast.12, bf16[352,4096]{1,0:T(8,128)(2,1)} %down_hbm.2, f32[32,128]{1,0:T(8,128)} %bitcast.15, f32[32,128]{1,0:T(8,128)} %bitcast.16, ...), custom_call_target="tpu_custom_call" | custom-call | tf_op jit(solution)/shard_map/first_block/pallas_call | solution.py:896
  47.5 0.0 copy-done
  47.5 0.0 copy-done.1
  47.5 0.0 copy-done.2
  47.5 3.8 %state_update.1 = (f32[8,16,128,128]{3,2,1,0:T(8,128)}, f32[128,128]{1,0:T(8,128)S(1)}) custom-call(f32[528,128]{1,0:T(8,128)S(1)} %get-tuple-element.6.refs_0_, f32[16,128]{1,0:T(8,128)S(1)} %bitcast.9, f32[1,128]{1,0:T(1,128)S(1)} %bitcast.10, f32[8,16,128,128]{3,2,1,0:T(8,128)S(1)} %copy-done), custom_call_target="tpu_custom_call" | custom-call | tf_op jit(solution)/shard_map/state_update/pallas_call | solution.py:933
  51.3 35.8 %second_block.1 = bf16[256,128]{1,0:T(8,128)(2,1)S(1)} custom-call(f32[128,128]{1,0:T(8,128)S(1)} %get-tuple-element.7.mixer_out, bf16[256,128]{1,0:T(8,128)(2,1)S(1)} %get-tuple-element.8.share_hbm, bf16[2048,128]{1,0:T(8,128)(2,1)} %output_hbm.1, bf16[352,4096]{1,0:T(8,128)(2,1)} %bitcast.13, bf16[352,4096]{1,0:T(8,128)(2,1)} %bitcast.14, ...), custom_call_target="tpu_custom_call" | custom-call | tf_op jit(solution)/shard_map/second_block/pallas_call | solution.py:953
  87.1 0.6 copy.21
Async XLA Ops:
  0.6 46.9 %copy-start = (f32[8,16,128,128]{3,2,1,0:T(8,128)S(1)}, f32[8,16,128,128]{3,2,1,0:T(8,128)}, u32[]{:S(2)}) copy-start(f32[8,16,128,128]{3,2,1,0:T(8,128)} %refs_3_.1) | copy-start | bytes 25165828
  0.6 46.9 %copy-start.1 = (f32[2048]{0:T(1024)S(1)}, f32[2048]{0:T(1024)}, u32[]{:S(2)}) copy-start(f32[2048]{0:T(1024)} %param.29) | copy-start | bytes 24580
  0.7 46.9 %copy-start.2 = (f32[128]{0:T(128)S(1)}, f32[128]{0:T(128)}, u32[]{:S(2)}) copy-start(f32[128]{0:T(128)} %param.30) | copy-start | bytes 1540

commit v6 on v5

--- a/solution.py
+++ b/solution.py
@@ -133,6 +133,7 @@
     copies = {}
     send = wire.sender(held.at[pl.ds(0, BLOCKS - 1)])
     crossing = {chips: wire.receiver() for chips in (IN_LINE, EARLY, LATE)}
+    aside = {chip: wire.receiver() for chip in EARLY + LATE}
 
     def view(half, first, second, core):
         start, rows, _ = halves[half]
@@ -150,6 +151,7 @@
                 axes_of(half)[stage],
                 step,
                 send,
+                aside.get(axes_chip(half, *chip)),
             )
 
     def crossed(half, first, second):
@@ -186,37 +188,38 @@
         blocks = held.at[pl.ds(KEPT_AT[(*chips[0], 1)], len(chips))]
         wire.receive(crossing[chips], blocks)
 
-    aside = [
-        (half, first, there)
-        for firsts, theres in (((1, 3), (1, 3)), ((1, 3), (2,)), ((2,), NEAR_FIRST))
-        for first in firsts
-        for there in theres
-        for half in both
-    ]
-    for half, first, there in aside:
-        copies[half, "across", first, there] = crossed(half, first, there)
-    early, late = aside[:8], aside[8:]
-
-    def pass_on(blocks):
-        for half, first, there in blocks:
-            arrive(half, 1, first, there)
-            copies[half, "across", first, there].start()
+    onward = {
+        chip: wire.prepare(
+            held.at[KEPT_AT[(*chip, 0)]],
+            held.at[KEPT_AT[(*chip, 1)]],
+            "tp",
+            1,
+            send,
+            crossing[EARLY if chip in EARLY else LATE],
+        )
+        for chip in aside
+    }
+
+    def pass_on(chips):
+        for chip in chips:
+            wire.receive(aside[chip], held.at[KEPT_AT[(*chip, 0)]])
+            onward[chip].start()
 
     if eager:
         @pl.when(wire.core == 1)
         def _():
-            pass_on(early)
+            pass_on(EARLY)
 
         settle(IN_LINE)
         ready(0)
 
         @pl.when(wire.core == 1)
         def _():
-            pass_on(late)
+            pass_on(LATE)
 
         @pl.when(wire.core == 0)
         def _():
-            pass_on(early)
+            pass_on(EARLY)
 
         ready(1)
         settle(EARLY)
@@ -224,10 +227,10 @@
 
         @pl.when(wire.core == 0)
         def _():
-            pass_on(late)
+            pass_on(LATE)
 
     else:
-        pass_on(early + late)
+        pass_on(EARLY + LATE)
         settle(IN_LINE)
         ready(0)
         ready(1)
@@ -904,7 +907,7 @@
         out_specs=in_space(VMEM, VMEM),
         scratch_shapes=[
             pltpu.SemaphoreType.DMA((21,)),
-            pltpu.SemaphoreType.DMA((86,)),
+            pltpu.SemaphoreType.DMA((77,)),
             *feed_forward_scratch(rows, full_width, hidden),
             pltpu.VMEM((2 * share, 2 * heads * keys), BF16),
             pltpu.VMEM((2 * share, 2 * heads * values), BF16),
@@ -958,7 +961,7 @@
         out_specs=pl.BlockSpec(memory_space=VMEM),
         scratch_shapes=[
             pltpu.SemaphoreType.DMA((8,)),
-            pltpu.SemaphoreType.DMA((78,)),
+            pltpu.SemaphoreType.DMA((60,)),
             *feed_forward_scratch(rows, full_width, hidden),
             pltpu.VMEM((BLOCKS, heads * seqs, LANES), BF16),
             pltpu.VMEM((heads * values // 2, 2 * LANES), BF16),

time: 88.1 us -> 87.7 us (level)
  no operation moved by 1% of the time
where the time goes in v6:
time: 87.7 us; the launch traced here: 87.6 us
  Pallas kernels  86.2 us (98%)
    pallas_call x1, Pallas kernels, per_device(): pl.pallas_call(first_kernel, name='first_block', out_shape=(jax.ShapeDtyp...  46.8 us
    pallas_call x1, Pallas kernels, per_device(): pl.pallas_call(second_kernel, name='second_block', out_shape=jax.ShapeDty...  35.7 us
    pallas_call x1, Pallas kernels, per_device(): pl.pallas_call(lambda *refs: state_kernel(full_width, *refs), name='state...  3.77 us

profile of v6, /device:TPU:0, one launch (start us, length us, event | category | flops | bytes accessed | tf_op | source)
XLA Modules:
  0.0 87.6 jit_solution(16102044563640780462)
XLA Ops:
  0.6 0.0 copy-start
  0.6 0.0 copy-start.1
  0.7 0.0 copy-start.2
  0.7 46.8 %first_block.1 = (f32[528,128]{1,0:T(8,128)S(1)}, bf16[256,128]{1,0:T(8,128)(2,1)S(1)}) custom-call(bf16[256,128]{1,0:T(8,128)(2,1)} %tokens.1, bf16[352,4096]{1,0:T(8,128)(2,1)} %bitcast.11, bf16[352,4096]{1,0:T(8,128)(2,1)} %bitcast.12, bf16[352,4096]{1,0:T(8,128)(2,1)} %down_hbm.2, f32[32,128]{1,0:T(8,128)} %bitcast.15, f32[32,128]{1,0:T(8,128)} %bitcast.16, ...), custom_call_target="tpu_custom_call" | custom-call | tf_op jit(solution)/shard_map/first_block/pallas_call | solution.py:899
  47.4 0.0 copy-done
  47.4 0.0 copy-done.1
  47.5 0.0 copy-done.2
  47.5 3.8 %state_update.1 = (f32[8,16,128,128]{3,2,1,0:T(8,128)}, f32[128,128]{1,0:T(8,128)S(1)}) custom-call(f32[528,128]{1,0:T(8,128)S(1)} %get-tuple-element.6.refs_0_, f32[16,128]{1,0:T(8,128)S(1)} %bitcast.9, f32[1,128]{1,0:T(1,128)S(1)} %bitcast.10, f32[8,16,128,128]{3,2,1,0:T(8,128)S(1)} %copy-done), custom_call_target="tpu_custom_call" | custom-call | tf_op jit(solution)/shard_map/state_update/pallas_call | solution.py:936
  51.2 35.7 %second_block.1 = bf16[256,128]{1,0:T(8,128)(2,1)S(1)} custom-call(f32[128,128]{1,0:T(8,128)S(1)} %get-tuple-element.7.mixer_out, bf16[256,128]{1,0:T(8,128)(2,1)S(1)} %get-tuple-element.8.share_hbm, bf16[2048,128]{1,0:T(8,128)(2,1)} %output_hbm.1, bf16[352,4096]{1,0:T(8,128)(2,1)} %bitcast.13, bf16[352,4096]{1,0:T(8,128)(2,1)} %bitcast.14, ...), custom_call_target="tpu_custom_call" | custom-call | tf_op jit(solution)/shard_map/second_block/pallas_call | solution.py:956
  86.9 0.6 copy.21
Async XLA Ops:
  0.6 46.8 %copy-start = (f32[8,16,128,128]{3,2,1,0:T(8,128)S(1)}, f32[8,16,128,128]{3,2,1,0:T(8,128)}, u32[]{:S(2)}) copy-start(f32[8,16,128,128]{3,2,1,0:T(8,128)} %refs_3_.1) | copy-start | bytes 25165828
  0.6 46.8 %copy-start.1 = (f32[2048]{0:T(1024)S(1)}, f32[2048]{0:T(1024)}, u32[]{:S(2)}) copy-start(f32[2048]{0:T(1024)} %param.29) | copy-start | bytes 24580
  0.7 46.8 %copy-start.2 = (f32[128]{0:T(128)S(1)}, f32[128]{0:T(128)}, u32[]{:S(2)}) copy-start(f32[128]{0:T(128)} %param.30) | copy-start | bytes 1540
